TPU v7x, 256 devices: a whole 4x4x8 slice. The times are simulated.
256 devices in a mesh: sp: 32 (over z, x), tp: 8 (over y, core).
Axes of the slice: x: 4, y: 4, z: 8, core: 2. Of those that a mesh axis runs over, the one named last changes fastest.
Arguments:
- out_grad: bfloat16 [4096, 2048], P('sp', 'tp'), may hold values from -6 to 6
- moe_input: bfloat16 [4096, 2048], P('sp', 'tp'), may hold values from -6 to 6
- route_weight: float32 [4096, 2], P('sp'), may hold values from 0.2 to 1
- route_ids: int32 [4096, 2], P('sp'), may hold values from 0 to 31, all different within a row; in each aligned block of 128 rows (0 to 127, 128 to 255, ...) at most 16 rows name the same one
- gate_proj: bfloat16 [32, 2048, 2816], P('sp', None, 'tp'), may hold values from -0.125 to 0.125
- up_proj: bfloat16 [32, 2048, 2816], P('sp', None, 'tp'), may hold values from -0.125 to 0.125
- down_proj: bfloat16 [32, 2816, 2048], P('sp', 'tp'), may hold values from -0.109375 to 0.109375
- out_proj: bfloat16 [2048, 2048], P(None, 'tp'), may hold values from -0.125 to 0.125
- conv_out: bfloat16 [4096, 2048], P('sp', 'tp'), may hold values from -6 to 6
- gate_b: bfloat16 [4096, 2048], P('sp', 'tp'), may hold values from -6 to 6
- gate_c: bfloat16 [4096, 2048], P('sp', 'tp'), may hold values from -6 to 6
- value_v: bfloat16 [4096, 2048], P('sp', 'tp'), may hold values from -6 to 6
- conv_taps: float32 [3, 2048], P(None, 'tp'), may hold values from -3 to 3
Outputs:
- grad_gate: bfloat16 [32, 2048, 2816], P('sp', None, 'tp')
- grad_up: bfloat16 [32, 2048, 2816], P('sp', None, 'tp')
- grad_down: bfloat16 [32, 2816, 2048], P('sp', 'tp')
- grad_out: float32 [2048, 2048], P('sp', 'tp')
- grad_b: bfloat16 [4096, 2048], P('sp', 'tp')
- grad_c: bfloat16 [4096, 2048], P('sp', 'tp')
- grad_v: bfloat16 [4096, 2048], P('sp', 'tp')
Inputs may be any that keep to these rules, and one draw needn't show every extreme that they name: `route_ids`: each row names two different experts; within the 128 rows of one index of sp no expert is named by more than 16 rows, a bound that some block reaches.
All inputs are finite; a program needn't handle non-finite values.
Results may differ from a plain program's by a relative error of at most 0.019.
Values may be sent and summed in bfloat16 or wider, within the bound.
A program may use at most 64 MiB of HBM per device.

v0:
```python
import jax
import jax.numpy as jnp
from jax import lax
from jax.sharding import Mesh
from jax.sharding import PartitionSpec as P

SP = ("sp_0", "sp_1")


def sent_together(arrays, axis, split_dim, concat_dim, along):
    ends, at = ([], 0)
    for a in arrays[:-1]:
        at += a.shape[along]
        ends.append(at)
    both = jnp.concatenate(arrays, axis=along)
    return tuple(
        jnp.split(
            lax.all_to_all(both, axis, split_axis=split_dim, concat_axis=concat_dim, tiled=True),
            ends,
            axis=along,
        )
    )


def in_one_piece(arrays, axis, dim, along):
    ends, at = ([], 0)
    for a in arrays[:-1]:
        at += a.shape[along]
        ends.append(at)
    both = jnp.concatenate(arrays, axis=along)
    return tuple(jnp.split(lax.all_gather(both, axis, axis=dim, tiled=True), ends, axis=along))


def cut_along(x, dim, peers):
    before, after = (x.shape[:dim], x.shape[dim + 1 :])
    return jnp.moveaxis(x.reshape(*before, peers, -1, *after), dim, 0)


def summed_on_arrival(x, axis, dim):
    blocks = cut_along(x, dim, lax.axis_size(axis))
    arrived = lax.all_to_all(blocks, axis, split_axis=0, concat_axis=0, tiled=True)
    return arrived.astype(jnp.float32).sum(axis=0)


def sent_to_all(x, axis):
    copies = jnp.broadcast_to(x, (lax.axis_size(axis), *x.shape))
    return lax.all_to_all(copies, axis, split_axis=0, concat_axis=0, tiled=True)


def laid_out(blocks, dim):
    blocks = jnp.moveaxis(blocks, 0, dim)
    shape = blocks.shape
    return blocks.reshape(*shape[:dim], shape[dim] * shape[dim + 1], *shape[dim + 2 :])


def collect(x, axis, dim):
    blocks = sent_to_all(x, axis)
    return laid_out(blocks, dim)


def with_halo(block, sides, width):
    for axis, dim in sides:
        count = lax.axis_size(axis)
        forward = [(i, i + 1) for i in range(count - 1)]
        backward = [(target, source) for source, target in forward]
        low = lax.ppermute(
            lax.slice_in_dim(block, block.shape[dim] - width, None, axis=dim), axis, forward
        )
        high = lax.ppermute(lax.slice_in_dim(block, 0, width, axis=dim), axis, backward)
        block = jnp.concatenate([low, block, high], axis=dim)
    return block


def cut_rows(length, count):
    unit = 8 if length >= 8 * count else 1
    return [length // unit * k // count * unit for k in range(1, count)]


def own_block(blocks, axes, sequence):
    inside = blocks.shape[1:]
    blocks = blocks.reshape(*(lax.axis_size(a) for a in axes), *inside)
    blocks = jnp.moveaxis(blocks, sequence, range(len(axes))).reshape(-1, *inside)
    for k in sequence:
        blocks = lax.psum_scatter(blocks, axes[k], scatter_dimension=0, tiled=True)
    return blocks[0]


def sum_at_once(x, axes, dim):
    blocks = cut_along(x, dim, lax.axis_size(axes))
    split_at = max(range(1, max(2, blocks.ndim - 1)), key=lambda d: blocks.shape[d])
    count, finished = (len(axes), [])
    for initial, section in enumerate(
        jnp.split(blocks, cut_rows(blocks.shape[split_at], count), axis=split_at)
    ):
        if section.size:
            sequence = [(initial + k) % count for k in range(count)]
            finished.append(own_block(section, axes, sequence))
    return jnp.concatenate(finished, axis=split_at - 1)


def place_rows(rows, index, total):
    return jnp.zeros((total, rows.shape[1]), rows.dtype).at[index].set(rows)


def local(
    out_grad,
    moe_input,
    route_weight,
    route_ids,
    gate_proj,
    up_proj,
    down_proj,
    out_proj,
    conv_out,
    gate_b,
    gate_c,
    value_v,
    conv_taps,
):
    tok_rows = out_grad.shape[0]
    local_cols = out_grad.shape[1]
    n_experts = lax.axis_size(SP)
    capacity = 4 * tok_rows // n_experts
    flat = route_ids.reshape(2 * tok_rows)
    onehot = (flat[:, None] == jnp.arange(n_experts, dtype=jnp.int32)[None, :]).astype(jnp.int32)
    before = jnp.cumsum(onehot, axis=0) - onehot
    slot = jnp.sum(before * onehot, axis=1)
    dest = flat * capacity + slot
    total = n_experts * capacity
    rows_x = jnp.broadcast_to(moe_input[:, None, :], (tok_rows, 2, local_cols)).reshape(
        2 * tok_rows, local_cols
    )
    rows_dy = (
        (route_weight[:, :, None] * out_grad.astype(jnp.float32)[:, None, :])
        .astype(jnp.bfloat16)
        .reshape(2 * tok_rows, local_cols)
    )
    send_x = place_rows(rows_x, dest, total).reshape(n_experts, capacity, local_cols)
    send_dy = place_rows(rows_dy, dest, total).reshape(n_experts, capacity, local_cols)
    part_x, part_dy = sent_together((send_x, send_dy), SP, 0, 0, 1)
    recv_x, recv_dy = in_one_piece((part_x, part_dy), "tp", 2, 0)
    width = recv_x.shape[2]
    xin = recv_x.reshape(total, width)
    dyin = recv_dy.reshape(total, width)
    w_gate = gate_proj[0]
    w_up = up_proj[0]
    w_down = down_proj[0]
    gate = jnp.dot(xin, w_gate, preferred_element_type=jnp.float32)
    upval = jnp.dot(xin, w_up, preferred_element_type=jnp.float32)
    sig = jax.nn.sigmoid(gate)
    act = gate * sig
    hidden = (act * upval).astype(jnp.bfloat16)
    grad_down = jnp.dot(hidden.T, dyin, preferred_element_type=jnp.float32).astype(jnp.bfloat16)
    dhid = jnp.dot(dyin, w_down.T, preferred_element_type=jnp.float32)
    dgate = (dhid * upval * (sig * (1.0 + gate * (1.0 - sig)))).astype(jnp.bfloat16)
    dup = (dhid * act).astype(jnp.bfloat16)
    grad_gate = jnp.dot(xin.T, dgate, preferred_element_type=jnp.float32).astype(jnp.bfloat16)
    grad_up = jnp.dot(xin.T, dup, preferred_element_type=jnp.float32).astype(jnp.bfloat16)
    partial_value = jnp.dot(dgate, w_gate.T, preferred_element_type=jnp.float32) + jnp.dot(
        dup, w_up.T, preferred_element_type=jnp.float32
    )
    partial_value = lax.optimization_barrier(partial_value.astype(jnp.bfloat16)).astype(jnp.float32)
    summed = summed_on_arrival(partial_value.astype(jnp.bfloat16), "tp", 1).astype(jnp.bfloat16)
    returned = lax.all_to_all(
        summed.reshape(n_experts, capacity, local_cols), SP, split_axis=0, concat_axis=0, tiled=True
    )
    picked = returned.reshape(total, local_cols)[dest]
    moe_grad = jnp.sum(picked.reshape(tok_rows, 2, local_cols).astype(jnp.float32), axis=1)
    grad_h = (out_grad.astype(jnp.float32) + moe_grad).astype(jnp.bfloat16)
    full_h = collect(grad_h, "tp", 1)
    grad_z = jnp.dot(full_h, out_proj, preferred_element_type=jnp.float32)
    dconv = (grad_z * gate_b.astype(jnp.float32)).astype(jnp.bfloat16)
    grad_b = (grad_z * conv_out.astype(jnp.float32)).astype(jnp.bfloat16)
    padded = with_halo(dconv, ((SP, 0),), 1).astype(jnp.float32)
    grad_u = conv_taps[0] * padded[2:] + conv_taps[1] * padded[1:-1] + conv_taps[2] * padded[:-2]
    grad_c = (grad_u * value_v.astype(jnp.float32)).astype(jnp.bfloat16)
    grad_v = (grad_u * gate_c.astype(jnp.float32)).astype(jnp.bfloat16)
    mixed = (gate_b.astype(jnp.float32) * conv_out.astype(jnp.float32)).astype(jnp.bfloat16)
    grad_out = sum_at_once(
        lax.dot_general(
            full_h, mixed, (((0,), (0,)), ((), ())), preferred_element_type=jnp.float32
        ).astype(jnp.bfloat16),
        SP,
        0,
    ).astype(jnp.float32)
    return (grad_gate[None], grad_up[None], grad_down[None], grad_out, grad_b, grad_c, grad_v)


def solution(mesh):
    split = Mesh(mesh.devices.reshape(8, 4, mesh.shape["tp"]), ("sp_0", "sp_1", "tp"))
    return jax.shard_map(
        local,
        mesh=split,
        in_specs=(
            P(SP, "tp"),
            P(SP, "tp"),
            P(SP, None),
            P(SP, None),
            P(SP, None, "tp"),
            P(SP, None, "tp"),
            P(SP, "tp", None),
            P(None, "tp"),
            P(SP, "tp"),
            P(SP, "tp"),
            P(SP, "tp"),
            P(SP, "tp"),
            P(None, "tp"),
        ),
        out_specs=(
            P(SP, None, "tp"),
            P(SP, None, "tp"),
            P(SP, "tp", None),
            P(SP, "tp"),
            P(SP, "tp"),
            P(SP, "tp"),
            P(SP, "tp"),
        ),
        check_vma=False,
    )
```

profile of v0, /device:TPU:1, one launch (start us, length us, event | category | flops | bytes accessed | tf_op | source)
XLA Modules:
  0.0 286.4 jit_solution(10276640265390173089)
XLA Ops:
  10.2 0.9 mul.109
  12.2 0.9 broadcast_in_dim.10
  13.3 1.5 scatter_custom_fusion
  14.8 1.6 scatter_custom_fusion.1
  16.5 27.9 %all_to_all.20 = bf16[32,32,256]{2,1,0:T(8,128)(2,1)S(1)} all-to-all(bf16[32,32,256]{2,1,0:T(8,128)(2,1)S(1)} %pad_maximum_fusion), channel_id=1, replica_groups=mesh['sp_0'=8,'sp_1'=4,'tp'=8] {'sp_0','sp_1'}, dimensions={0} | all-to-all | bytes 1048576 | tf_op jit(solution)/shard_map/all_to_all | solution.py:18
  45.4 36.7 %all-gather.2.cloned.1.call-done = bf16[64,16,2048]{2,1,0:T(8,128)(2,1)} async-done(((bf16[64,16,256]{2,1,0:T(8,128)(2,1)}), bf16[64,16,2048]{2,1,0:T(8,128)(2,1)}) %all-gather.2.cloned.1.call-update) | async-done | bytes 4194320 | tf_op jit(solution)/shard_map/all_gather | solution.py:31
  82.1 2.7 fusion.31
  84.9 1.0 fusion.5
  86.2 1.1 copy-done.4
  87.3 1.0 fusion.8
  88.9 1.2 multiply_convert_fusion.1
  90.1 1.3 fusion.3
  91.4 1.4 add_convert_fusion
  92.9 30.2 %all_to_all.21 = bf16[8,512,256]{2,1,0:T(8,128)(2,1)S(1)} all-to-all(bf16[8,512,256]{2,1,0:T(8,128)(2,1)S(1)} %bitcast.81), channel_id=1, replica_groups=mesh['sp_0'=8,'sp_1'=4,'tp'=8] {'tp'}, dimensions={0} | all-to-all | bytes 4194304 | tf_op jit(solution)/shard_map/all_to_all | solution.py:41
  123.1 1.1 reduce_sum.34
  124.2 9.7 %all-to-all-start.2 = ((bf16[32,16,256]{2,1,0:T(8,128)(2,1)}), bf16[32,16,256]{2,1,0:T(8,128)(2,1)S(1)}, u32[]{:S(2)}, u32[]{:S(2)}) async-start(bf16[32,16,256]{2,1,0:T(8,128)(2,1)} %bitcast.95), calls=%async_computation.2 | async-start | bytes 524288 | tf_op jit(solution)/shard_map/all_to_all | solution.py:164
  133.9 10.5 %all-to-all-done.2 = bf16[32,16,256]{2,1,0:T(8,128)(2,1)S(1)} async-done(((bf16[32,16,256]{2,1,0:T(8,128)(2,1)}), bf16[32,16,256]{2,1,0:T(8,128)(2,1)S(1)}, u32[]{:S(2)}, u32[]{:S(2)}) %all-to-all-start.2) | async-done | bytes 262176 | tf_op jit(solution)/shard_map/all_to_all | solution.py:164
  144.5 1.2 gather_fusion
  146.3 14.7 %all_to_all.22 = bf16[8,128,256]{1,2,0:T(8,128)(2,1)S(1)} all-to-all(bf16[8,128,256]{1,2,0:T(8,128)(2,1)S(1)} %broadcast_in_dim.28), channel_id=1, replica_groups=mesh['sp_0'=8,'sp_1'=4,'tp'=8] {'tp'}, dimensions={0} | all-to-all | bytes 1048576 | tf_op jit(solution)/shard_map/all_to_all | solution.py:47
  161.5 0.9 fusion.32
  162.5 0.8 copy.35
  163.4 3.8 %fusion.1 = bf16[1,2048,352]{1,2,0:T(8,128)(2,1)} fusion(bf16[512,352]{0,1:T(8,128)(2,1)S(1)} %copy-done.7, bf16[512,2048]{1,0:T(8,128)(2,1)} %bitcast.91), kind=kOutput, calls=%fused_computation.9 | convolution fusion | flops 738918400 | bytes 3899392 | tf_op jit(solution)/shard_map/dot_general | solution.py:157
  167.2 2.1 fusion
  169.3 1.0 fusion.13
  170.3 1.3 collective-permute-start.1
  171.6 4.0 %collective-permute-start = (bf16[1,256]{1,0:T(2,128)(2,1)S(1)}, bf16[1,256]{1,0:T(2,128)(2,1)S(1)}, u32[]{:S(2)}, u32[]{:S(2)}) collective-permute-start(bf16[1,256]{1,0:T(2,128)(2,1)S(1)} %get-tuple-element.19), channel_id=1, source_target_pairs={{0,8},{8,16},{16,24},{24,32},{32,40},{40,48},{48,56},{56,64},{64,7... | collective-permute-start | bytes 1544 | tf_op jit(solution)/shard_map/ppermute | solution.py:66
  175.6 14.0 %reduce-scatter.5.cloned.1.call-done = bf16[4,32,256]{2,1,0:T(8,128)(2,1)} async-done(((bf16[32,32,256]{2,1,0:T(8,128)(2,1)}), bf16[4,32,256]{2,1,0:T(8,128)(2,1)}) %reduce-scatter.5.cloned.1.call-update) | async-done | bytes 65552 | tf_op jit(solution)/shard_map/reduce_scatter | solution.py:84
  189.7 3.6 %fusion.2 = bf16[1,2048,352]{1,2,0:T(8,128)(2,1)} fusion(bf16[512,352]{0,1:T(8,128)(2,1)S(1)} %copy-done.9, bf16[512,2048]{1,0:T(8,128)(2,1)} %bitcast.92), kind=kOutput, calls=%fused_computation.10 | convolution fusion | flops 738918400 | bytes 3899392 | tf_op jit(solution)/shard_map/dot_general | solution.py:158
  193.3 24.0 %reduce-scatter.9.cloned.1.call-done = bf16[8,32,256]{2,1,0:T(8,128)(2,1)} async-done(((bf16[32,32,256]{2,1,0:T(8,128)(2,1)}), bf16[8,32,256]{2,1,0:T(8,128)(2,1)}) %reduce-scatter.9.cloned.1.call-update) | async-done | bytes 131088 | tf_op jit(solution)/shard_map/reduce_scatter | solution.py:84
  218.7 23.9 %reduce-scatter.7.cloned.1.call-done = bf16[1,32,256]{2,1,0:T(8,128)(2,1)} async-done(((bf16[4,32,256]{2,1,0:T(8,128)(2,1)}), bf16[1,32,256]{2,1,0:T(8,128)(2,1)}) %reduce-scatter.7.cloned.1.call-update) | async-done | bytes 16400 | tf_op jit(solution)/shard_map/reduce_scatter | solution.py:84
  242.6 35.9 %reduce-scatter.11.cloned.1.call-done = bf16[1,32,256]{2,1,0:T(8,128)(2,1)} async-done(((bf16[8,32,256]{2,1,0:T(8,128)(2,1)}), bf16[1,32,256]{2,1,0:T(8,128)(2,1)}) %reduce-scatter.11.cloned.1.call-update) | async-done | bytes 16400 | tf_op jit(solution)/shard_map/reduce_scatter | solution.py:84
  278.5 1.4 maximum_convert_fusion.1
  (86 shorter events, 9.0 us)
Async XLA Ops:
  7.2 77.7 %copy-start = (bf16[1,2048,352]{1,2,0:T(8,128)(2,1)S(1)}, bf16[1,2048,352]{1,2,0:T(8,128)(2,1)}, u32[]{:S(2)}) copy-start(bf16[1,2048,352]{1,2,0:T(8,128)(2,1)} %param.17) | copy-start | bytes 4325380
  7.2 74.9 %all-gather.2.cloned.1.call-start = ((), (), s32[]{:S(2)}) async-start(), calls=%async_computation.8 | async-start | bytes 4718592 | tf_op jit(solution)/shard_map/all_gather | solution.py:31
  84.8 1.3 copy-start.1
  84.8 3.4 %copy-start.2 = (bf16[32,16,2048]{2,1,0:T(8,128)(2,1)}, bf16[32,16,2048]{2,1,0:T(8,128)(2,1)S(1)}, u32[]{:S(2)}) copy-start(bf16[32,16,2048]{2,1,0:T(8,128)(2,1)S(1)} %get-tuple-element.9) | copy-start | bytes 6291460
  84.8 2.4 copy-start.4
  87.3 1.0 copy-start.17
  87.3 1.6 copy-start.16
  88.3 1.8 copy-start.19
  90.1 1.3 copy-start.6
  90.1 1.3 copy-start.8
  124.2 21.9 %copy-start.10 = (bf16[128,256]{1,0:T(8,128)(2,1)S(1)}, bf16[128,256]{1,0:T(8,128)(2,1)}, u32[]{:S(2)}) copy-start(bf16[128,256]{1,0:T(8,128)(2,1)} %param.13) | copy-start | bytes 196612
  124.2 20.3 %all-to-all-start.2 = ((bf16[32,16,256]{2,1,0:T(8,128)(2,1)}), bf16[32,16,256]{2,1,0:T(8,128)(2,1)S(1)}, u32[]{:S(2)}, u32[]{:S(2)}) async-start(bf16[32,16,256]{2,1,0:T(8,128)(2,1)} %bitcast.95), calls=%async_computation.2 | async-start | bytes 524288 | tf_op jit(solution)/shard_map/all_to_all | solution.py:164
  133.8 27.2 %copy-start.11 = (bf16[128,256]{1,0:T(8,128)(2,1)S(1)}, bf16[128,256]{1,0:T(8,128)(2,1)}, u32[]{:S(2)}) copy-start(bf16[128,256]{1,0:T(8,128)(2,1)} %param.21) | copy-start | bytes 196612
  133.9 27.2 %copy-start.12 = (bf16[128,256]{1,0:T(8,128)(2,1)S(1)}, bf16[128,256]{1,0:T(8,128)(2,1)}, u32[]{:S(2)}) copy-start(bf16[128,256]{1,0:T(8,128)(2,1)} %param.22) | copy-start | bytes 196612
  133.9 55.7 %reduce-scatter.5.cloned.1.call-start = ((), (), s32[]{:S(2)}) async-start(), calls=%async_computation.9 | async-start | bytes 589824 | tf_op jit(solution)/shard_map/reduce_scatter | solution.py:84
  161.1 1.4 copy-start.15
  161.5 1.9 copy-start.7
  162.4 54.9 %reduce-scatter.9.cloned.1.call-start = ((), (), s32[]{:S(2)}) async-start(), calls=%async_computation.11 | async-start | bytes 655360 | tf_op jit(solution)/shard_map/reduce_scatter | solution.py:84
  163.3 79.2 %reduce-scatter.7.cloned.1.call-start = ((), (), s32[]{:S(2)}) async-start(), calls=%async_computation.10 | async-start | bytes 81920 | tf_op jit(solution)/shard_map/reduce_scatter | solution.py:84
  163.4 3.8 %copy-start.3 = (bf16[32,16,2048]{2,1,0:T(8,128)(2,1)S(1)}, bf16[32,16,2048]{2,1,0:T(8,128)(2,1)}, u32[]{:S(2)}) copy-start(bf16[32,16,2048]{2,1,0:T(8,128)(2,1)} %copy-done.2) | copy-start | bytes 6291460
  163.4 3.8 %copy-start.18 = (f32[512,352]{0,1:T(8,128)S(1)}, f32[512,352]{0,1:T(8,128)}, u32[]{:S(2)}) copy-start(f32[512,352]{0,1:T(8,128)} %copy-done.17) | copy-start | bytes 2162692
  163.4 3.8 %copy-start.20 = (f32[512,352]{0,1:T(8,128)S(1)}, f32[512,352]{0,1:T(8,128)}, u32[]{:S(2)}) copy-start(f32[512,352]{0,1:T(8,128)} %copy-done.19) | copy-start | bytes 2162692
  167.2 2.1 copy-start.5
  167.2 22.5 %copy-start.9 = (bf16[512,352]{0,1:T(8,128)(2,1)S(1)}, bf16[512,352]{0,1:T(8,128)(2,1)}, u32[]{:S(2)}) copy-start(bf16[512,352]{0,1:T(8,128)(2,1)} %copy-done.8) | copy-start | bytes 1081348
  170.3 23.0 %collective-permute-start.1 = (bf16[1,256]{1,0:T(2,128)(2,1)S(1)}, bf16[1,256]{1,0:T(2,128)(2,1)S(1)}, u32[]{:S(2)}, u32[]{:S(2)}) collective-permute-start(bf16[1,256]{1,0:T(2,128)(2,1)S(1)} %get-tuple-element.20), channel_id=1, source_target_pairs={{8,0},{16,8},{24,16},{32,24},{40,32},{48,40},{56,48},{64,56},{72,6... | collective-permute-start | bytes 1544 | tf_op jit(solution)/shard_map/ppermute | solution.py:69
  171.6 21.7 %collective-permute-start = (bf16[1,256]{1,0:T(2,128)(2,1)S(1)}, bf16[1,256]{1,0:T(2,128)(2,1)S(1)}, u32[]{:S(2)}, u32[]{:S(2)}) collective-permute-start(bf16[1,256]{1,0:T(2,128)(2,1)S(1)} %get-tuple-element.19), channel_id=1, source_target_pairs={{0,8},{8,16},{16,24},{24,32},{32,40},{40,48},{48,56},{56,64},{64,7... | collective-permute-start | bytes 1544 | tf_op jit(solution)/shard_map/ppermute | solution.py:66
  189.6 27.7 %copy-start.13 = (bf16[128,256]{1,0:T(8,128)(2,1)S(1)}, bf16[128,256]{1,0:T(8,128)(2,1)}, u32[]{:S(2)}) copy-start(bf16[128,256]{1,0:T(8,128)(2,1)} %param.23) | copy-start | bytes 196612
  189.6 28.4 %copy-start.14 = (bf16[128,256]{1,0:T(8,128)(2,1)S(1)}, bf16[128,256]{1,0:T(8,128)(2,1)}, u32[]{:S(2)}) copy-start(bf16[128,256]{1,0:T(8,128)(2,1)} %param.24) | copy-start | bytes 196612
  189.6 88.8 %reduce-scatter.11.cloned.1.call-start = ((), (), s32[]{:S(2)}) async-start(), calls=%async_computation.12 | async-start | bytes 147456 | tf_op jit(solution)/shard_map/reduce_scatter | solution.py:84
Sparse Core Ops, SparseCore 0:
  45.5 36.5 all-gather.1
  162.5 27.0 reduce-scatter.4
  192.1 25.1 reduce-scatter.8
  219.6 22.8 reduce-scatter.6
  244.9 33.4 reduce-scatter.10
where the time goes:
time: 292 us; the launch traced here: 286 us
  waiting for transfers between devices  145 us (50%)
  blocking collectives  72.9 us (25%)
  matrix products  16.7 us (6%)
  starting transfers between devices  15.1 us (5%)
  local copies, waits for them, and re-layouts  14.3 us (5%)
  between operations  14.2 us (5%)
  other arithmetic  8.14 us (3%)
    reduce_scatter x4, waiting for transfers between devices, own_block(): blocks = lax.psum_scatter(blocks, axes[k], scatter_dimension=0, tiled=True)  97.7 us
    all_gather x1, waiting for transfers between devices, in_one_piece(): lax.all_gather(both, axis, axis=dim, tiled=True)  36.7 us
    all_to_all x1, blocking collectives, summed_on_arrival(): lax.all_to_all(blocks, axis, split_axis=0, concat_axis=0, tiled=True)  30.2 us
    all_to_all x1, blocking collectives, sent_together(): lax.all_to_all(both, axis, split_axis=split_dim, concat_axis=concat_dim,...  27.9 us
    all_to_all x1, blocking collectives, sent_to_all(): return lax.all_to_all(copies, axis, split_axis=0, concat_axis=0, tiled=True)  14.7 us
    all_to_all x1, waiting for transfers between devices, local(): lax.all_to_all(summed.reshape(n_experts, capacity, local_cols), SP, split...  10.5 us
    all_to_all x1, starting transfers between devices, local(): lax.all_to_all(summed.reshape(n_experts, capacity, local_cols), SP, split...  9.67 us
  transfers between devices with their start and end apart: 8, of which 6 were waited for; matrix products, arithmetic and copies ran while one was open for 4% of the time, Pallas kernels for 0%

commit v1 on v0

v1 whole, which is shorter than its diff:
```python
import functools

import jax
import jax.numpy as jnp
from jax import lax
from jax.experimental import pallas as pl
from jax.experimental.pallas import tpu as pltpu
from jax.sharding import PartitionSpec as P

MESH = pl.DeviceIdType.MESH
NX = 4
NY = 4
BF = jnp.bfloat16
F32 = jnp.float32


def block_order(nz):
    order = [0]
    for d in range(1, nz // 2 + 1):
        order.append(d)
        if nz - d != d:
            order.append(nz - d)
    return order[:nz]


class Place:
    def __init__(self, nz):
        self.nz = nz
        self.sp = lax.axis_index("sp")
        self.tp = lax.axis_index("tp")
        self.z = lax.div(self.sp, NX)
        self.x = lax.rem(self.sp, NX)
        self.y = lax.div(self.tp, 2)
        self.c = lax.rem(self.tp, 2)

    def over_sp(self, dz, dx):
        z = lax.rem(self.z + dz, self.nz)
        x = lax.rem(self.x + dx, NX)
        return (z * NX + x, self.tp)

    def over_y(self, dy):
        return (self.sp, lax.rem(self.y + dy + NY, NY) * 2 + self.c)

    def other(self):
        return (self.sp, self.y * 2 + 1 - self.c)

    def origin(self, dy, flip):
        y = lax.rem(self.y + dy + NY, NY)
        c = 1 - self.c if flip else self.c
        return y * 2 + c


def greet(here):
    barrier = pltpu.get_barrier_semaphore()
    peers = [here.over_sp(dz, dx) for dz in range(here.nz) for dx in range(NX) if dz or dx]
    peers += [here.other(), here.over_y(1), here.over_y(-1)]
    for peer in peers:
        pl.semaphore_signal(barrier, inc=1, device_id=peer, device_id_type=MESH)
    return barrier, len(peers)


def send(src, dst, send_sem, recv_sem, peer):
    copy = pltpu.make_async_remote_copy(
        src_ref=src,
        dst_ref=dst,
        send_sem=send_sem,
        recv_sem=recv_sem,
        device_id=peer,
        device_id_type=MESH,
    )
    copy.start()


def await_bytes(ref, sem):
    pltpu.make_async_copy(ref, ref, sem).wait()


class Gather:
    def __init__(self, here, chunk, send_sem, near, far):
        self.here, self.chunk, self.send_sem, self.near, self.far = here, chunk, send_sem, near, far

    def _send(self, origin, h, peer, recv_sem):
        ref = self.chunk(origin, h)
        send(ref, ref, self.send_sem, recv_sem, peer)

    def start(self, h):
        here = self.here
        mine = here.origin(0, False)
        self._send(mine, h, here.over_y(1), self.near.at[0, h])
        self._send(mine, h, here.over_y(-1), self.near.at[1, h])
        self._send(mine, h, here.other(), self.far.at[0])

    def forward(self, h):
        here = self.here
        low, high = here.origin(-1, False), here.origin(1, False)
        await_bytes(self.chunk(low, h), self.near.at[0, h])
        if h % 2 == 0:
            self._send(low, h, here.over_y(1), self.near.at[2, h])
        self._send(low, h, here.other(), self.far.at[1])
        await_bytes(self.chunk(high, h), self.near.at[1, h])
        if h % 2 == 1:
            self._send(high, h, here.over_y(-1), self.near.at[2, h])
        self._send(high, h, here.other(), self.far.at[2])

    def last(self, h):
        here = self.here
        across = here.origin(2, False)
        await_bytes(self.chunk(across, h), self.near.at[2, h])
        self._send(across, h, here.other(), self.far.at[3])

    def finish(self, whole):
        here = self.here
        for k, dy in enumerate((0, -1, 1, 2)):
            await_bytes(whole(here.origin(dy, True)), self.far.at[k])


def slots_of(ids, here, total):
    tokens = ids.shape[0]
    lanes = lax.broadcasted_iota(jnp.int32, (tokens, 128), 1)
    named = [(lanes == ids[:, k : k + 1]).astype(F32) for k in range(2)]
    rows = lax.broadcasted_iota(jnp.int32, (tokens, tokens), 0)
    cols = lax.broadcasted_iota(jnp.int32, (tokens, tokens), 1)
    earlier = (cols < rows).astype(F32).astype(BF)
    before = jnp.dot(earlier, (named[0] + named[1]).astype(BF), preferred_element_type=F32)
    cap = total // (here.nz * NX)
    out = []
    for k in range(2):
        slot = jnp.sum(before * named[k], axis=1, keepdims=True)
        e = ids[:, k : k + 1]
        dz = ((e // NX if NX not in (1, 2, 4) else (e >> (NX.bit_length() - 1))) - here.z) & (here.nz - 1)
        dx = ((e & (NX - 1)) - here.x) & (NX - 1)
        out.append(((dz * NX + dx) * cap).astype(F32) + slot)
    return out


def dispatch_kernel(
    nz, og_ref, x_ref, rw_ref, ids_ref, buf, sbuf, barrier_dummy, own_sem, sp_send, sp_recv, tp_send, near, far
):
    del barrier_dummy
    here = Place(nz)
    barrier, peers = greet(here)
    total, chans = sbuf.shape[1:]
    cap = total // (nz * NX)
    tokens = og_ref.shape[0]

    slots = slots_of(ids_ref[...], here, total)
    srow = lax.broadcasted_iota(jnp.int32, (total, tokens), 0).astype(F32)
    places = []
    for k in range(2):
        wide = jnp.broadcast_to(slots[k], (tokens, tokens)).T
        places.append((srow == wide[0:1, :]).astype(F32))
    both = (places[0] + places[1]).astype(BF)
    sbuf[0] = jnp.dot(both, x_ref[...], preferred_element_type=F32).astype(BF)
    og = og_ref[...].astype(F32)
    dy = None
    for k in range(2):
        weighted = (rw_ref[:, k : k + 1] * og).astype(BF)
        term = jnp.dot(places[k].astype(BF), weighted, preferred_element_type=F32)
        dy = term if dy is None else dy + term
    sbuf[1] = dy.astype(BF)

    order = block_order(nz)
    at = {d: p for p, d in enumerate(order)}
    rows = NX * cap
    column = pl.ds(pl.multiple_of(here.tp * chans, chans), chans)
    pl.semaphore_wait(barrier, peers)
    own = pltpu.make_async_copy(sbuf.at[:, 0:cap, :], buf.at[:, 0:cap, column], own_sem)
    own.start()
    for dz in order:
        for dx in range(NX):
            if dz or dx:
                r = (dz * NX + dx) * cap
                p = at[(-dz) % nz]
                t = p * rows + ((-dx) % NX) * cap
                send(
                    sbuf.at[:, pl.ds(r, cap), :],
                    buf.at[:, pl.ds(t, cap), column],
                    sp_send,
                    sp_recv.at[p],
                    here.over_sp(dz, dx),
                )

    def chunk(origin, h):
        return buf.at[:, pl.ds(h * rows, rows), pl.ds(pl.multiple_of(origin * chans, chans), chans)]

    def whole(origin):
        return buf.at[:, :, pl.ds(pl.multiple_of(origin * chans, chans), chans)]

    gather = Gather(here, chunk, tp_send, near, far)
    for p in range(nz + 2):
        if p < nz:
            if p == 0:
                own.wait()
                await_bytes(buf.at[:, cap:rows, column], sp_recv.at[0])
            else:
                await_bytes(buf.at[:, pl.ds(p * rows, rows), column], sp_recv.at[p])
            gather.start(p)
        if 0 <= p - 1 < nz:
            gather.forward(p - 1)
        if 0 <= p - 2 < nz:
            gather.last(p - 2)
    gather.finish(whole)
    await_bytes(sbuf.at[:, pl.ds(0, total - cap), :], sp_send)
    await_bytes(buf.at[:, pl.ds(0, total - total // (2 * NY)), :], tp_send)


def tail_kernel(
    nz,
    part_ref,
    og_ref,
    ids_ref,
    out_proj_ref,
    conv_ref,
    gb_ref,
    gc_ref,
    vv_ref,
    taps_ref,
    go_ref,
    gradb_ref,
    gradc_ref,
    gradv_ref,
    pr,
    sb,
    ra,
    rb,
    sc,
    rc,
    fin,
    ret,
    dh,
    dhall,
    dht,
    xb,
    xall,
    mixed,
    mx,
    edge,
    halo,
    gpart,
    gr,
    own_sem,
    pair_send,
    pair_recv,
    rs_send,
    rs_recv,
    sp_send,
    sp_recv,
    dh_send,
    dh_near,
    dh_far,
    xb_send,
    xb_near,
    xb_far,
    x_send,
    x_recv,
    m_send,
    m_recv,
    e_send,
    e_recv,
    z_send,
    z_recv,
):
    here = Place(nz)
    barrier, peers = greet(here)
    total = part_ref.shape[0]
    cap = total // (nz * NX)
    rows = NX * cap
    tokens, chans = og_ref.shape
    order = block_order(nz)
    half = total // 2

    slots = slots_of(ids_ref[...], here, total)
    scol = lax.broadcasted_iota(jnp.int32, (tokens, total), 1).astype(F32)
    pick = ((scol == slots[0]).astype(F32) + (scol == slots[1]).astype(F32)).astype(BF)
    mixed[...] = (gb_ref[...].astype(F32) * conv_ref[...].astype(F32)).astype(BF)
    pl.semaphore_wait(barrier, peers)

    for k in (1, 0):
        for y in range(NY):
            col = pl.ds(pl.multiple_of((2 * y + 1 - here.c) * chans, chans), chans)
            send(
                part_ref.at[pl.ds(k * half, half), col],
                pr.at[y, pl.ds(k * half, half), :],
                pair_send,
                pair_recv.at[k],
                here.other(),
            )
    mrow = pl.ds(pl.multiple_of(here.x * tokens, tokens), tokens)
    own_mixed = pltpu.make_async_copy(mixed, mx.at[mrow, :], own_sem.at[0])
    own_mixed.start()
    for dx in range(1, NX):
        send(mixed, mx.at[mrow, :], m_send, m_recv, here.over_sp(0, dx))

    def pair(p, dy):
        y = lax.rem(here.y + dy + NY, NY)
        r = pl.ds(p * rows, rows)
        col = pl.ds(pl.multiple_of((2 * y + here.c) * chans, chans), chans)
        return part_ref[r, col].astype(F32) + pr[y, r, :].astype(F32)

    def stage_a(p):
        way = 1 if p % 2 == 0 else -1
        r = pl.ds(p * rows, rows)
        if p == nz - 1:
            await_bytes(pr.at[:, pl.ds(half, half), :], pair_recv.at[1])
        if p == nz // 2 - 1:
            await_bytes(pr.at[:, pl.ds(0, half), :], pair_recv.at[0])
        sb[0, r, :] = pair(p, 2).astype(BF)
        send(sb.at[0, r, :], ra.at[r, :], rs_send.at[0], rs_recv.at[0, p], here.over_y(way))
        sb[1, r, :] = pair(p, -way).astype(BF)
        send(sb.at[1, r, :], rb.at[r, :], rs_send.at[1], rs_recv.at[1, p], here.over_y(-way))

    def stage_b(p):
        way = 1 if p % 2 == 0 else -1
        r = pl.ds(p * rows, rows)
        await_bytes(ra.at[r, :], rs_recv.at[0, p])
        sc[r, :] = (pair(p, way) + ra[r, :].astype(F32)).astype(BF)
        send(sc.at[r, :], rc.at[r, :], rs_send.at[2], rs_recv.at[2, p], here.over_y(way))

    def stage_c(p):
        r = pl.ds(p * rows, rows)
        await_bytes(rb.at[r, :], rs_recv.at[1, p])
        await_bytes(rc.at[r, :], rs_recv.at[2, p])
        fin[r, :] = (pair(p, 0) + rb[r, :].astype(F32) + rc[r, :].astype(F32)).astype(BF)
        dz = order[p]
        for dx in range(NX):
            src = fin.at[pl.ds(p * rows + dx * cap, cap), :]
            t = (((-dz) % nz) * NX + (-dx) % NX) * cap
            dst = ret.at[pl.ds(t, cap), :]
            if dz or dx:
                send(src, dst, sp_send, sp_recv, here.over_sp(dz, dx))

    for s in range(nz + 2):
        if s < nz:
            stage_a(nz - 1 - s)
        if 0 <= s - 1 < nz:
            stage_b(nz - s)
        if 0 <= s - 2 < nz:
            stage_c(nz + 1 - s)
    ret[0:cap, :] = fin[0:cap, :]
    await_bytes(ret.at[pl.ds(cap, total - cap), :], sp_recv)

    moe = jnp.dot(pick, ret[...], preferred_element_type=F32)
    grad_h = og_ref[...].astype(F32) + moe
    dht[...] = grad_h.T.astype(BF)
    dh[...] = grad_h.astype(BF)

    wide = chans // NX
    tcol = pl.ds(pl.multiple_of(here.x * tokens, tokens), tokens)
    block = pl.ds(pl.multiple_of(here.tp * wide, wide), wide)
    for dx in range(1, NX):
        to = lax.rem(here.x + dx, NX)
        send(
            dht.at[pl.ds(pl.multiple_of(to * wide, wide), wide), :],
            xb.at[:, tcol],
            x_send,
            x_recv,
            here.over_sp(0, dx),
        )
    own_x = pltpu.make_async_copy(
        dht.at[pl.ds(pl.multiple_of(here.x * wide, wide), wide), :], xb.at[:, tcol], own_sem.at[1]
    )
    own_x.start()
    hcol = pl.ds(pl.multiple_of(here.tp * chans, chans), chans)
    own_dh = pltpu.make_async_copy(dh, dhall.at[:, hcol], own_sem.at[2])
    own_dh.start()
    own_dh.wait()

    def dh_chunk(origin, h):
        return dhall.at[
            pl.ds(h * (tokens // 2), tokens // 2), pl.ds(pl.multiple_of(origin * chans, chans), chans)
        ]

    def dh_whole(origin):
        return dhall.at[:, pl.ds(pl.multiple_of(origin * chans, chans), chans)]

    def xb_chunk(origin, h):
        return xall.at[pl.ds(pl.multiple_of(origin * wide + h * (wide // 2), wide // 2), wide // 2), :]

    def xb_whole(origin):
        return xall.at[pl.ds(pl.multiple_of(origin * wide, wide), wide), :]

    dh_gather = Gather(here, dh_chunk, dh_send, dh_near, dh_far)
    xb_gather = Gather(here, xb_chunk, xb_send, xb_near, xb_far)
    dh_gather.start(0)
    dh_gather.start(1)
    own_x.wait()
    await_bytes(xb.at[:, pl.ds(0, (NX - 1) * tokens)], x_recv)
    place_x = pltpu.make_async_copy(xb, xall.at[block, :], own_sem.at[3])
    place_x.start()
    place_x.wait()
    xb_gather.start(0)
    xb_gather.start(1)
    for h in range(2):
        dh_gather.forward(h)
    for h in range(2):
        xb_gather.forward(h)
    for h in range(2):
        dh_gather.last(h)
    for h in range(2):
        xb_gather.last(h)
    dh_gather.finish(dh_whole)
    grad_z = jnp.dot(dhall[...], out_proj_ref[...], preferred_element_type=F32)
    dconv = (grad_z * gb_ref[...].astype(F32)).astype(BF)
    edge[0, :, :] = dconv[0:16, :]
    edge[1, :, :] = dconv[tokens - 16 :, :]
    last_sp = nz * NX
    before = (lax.rem(here.sp + last_sp - 1, last_sp), here.tp)
    after = (lax.rem(here.sp + 1, last_sp), here.tp)
    send(edge.at[0], halo.at[1], e_send.at[0], e_recv.at[1], before)
    send(edge.at[1], halo.at[0], e_send.at[1], e_recv.at[0], after)
    gradb_ref[...] = (grad_z * conv_ref[...].astype(F32)).astype(BF)

    own_mixed.wait()
    await_bytes(mx.at[pl.ds(0, (NX - 1) * tokens), :], m_recv)
    xb_gather.finish(xb_whole)
    gpart[...] = jnp.dot(xall[...], mx[...], preferred_element_type=F32).astype(BF)
    for dz in range(1, nz):
        to = lax.rem(here.z + dz, nz)
        send(
            gpart.at[pl.ds(pl.multiple_of(to * wide, wide), wide), :],
            gr.at[dz],
            z_send,
            z_recv,
            here.over_sp(dz, 0),
        )
    own_g = pltpu.make_async_copy(
        gpart.at[pl.ds(pl.multiple_of(here.z * wide, wide), wide), :], gr.at[0], own_sem.at[4]
    )
    own_g.start()

    await_bytes(halo.at[0], e_recv.at[0])
    await_bytes(halo.at[1], e_recv.at[1])
    dconv = dconv.astype(F32)
    row = lax.broadcasted_iota(jnp.int32, dconv.shape, 0)
    low = halo[0].astype(F32)[15:16, :] * (here.sp > 0).astype(F32)
    high = halo[1].astype(F32)[0:1, :] * (here.sp < last_sp - 1).astype(F32)
    prev = jnp.where(row == 0, low, pltpu.roll(dconv, 1, 0))
    nxt = jnp.where(row == tokens - 1, high, pltpu.roll(dconv, tokens - 1, 0))
    grad_u = taps_ref[0:1, :] * nxt + taps_ref[1:2, :] * dconv + taps_ref[2:3, :] * prev
    gradc_ref[...] = (grad_u * vv_ref[...].astype(F32)).astype(BF)
    gradv_ref[...] = (grad_u * gc_ref[...].astype(F32)).astype(BF)

    own_g.wait()
    await_bytes(gr.at[pl.ds(1, nz - 1)], z_recv)
    summed = gr[0].astype(F32)
    for k in range(1, nz):
        summed = summed + gr[k].astype(F32)
    go_ref[...] = summed

    await_bytes(pr, pair_send)
    for k in range(3):
        await_bytes(ra, rs_send.at[k])
    await_bytes(ret.at[pl.ds(cap, total - cap), :], sp_send)
    await_bytes(dhall.at[:, pl.ds(0, (2 * NY - 1) * chans)], dh_send)
    await_bytes(xall.at[pl.ds(0, (2 * NY - 1) * wide), :], xb_send)
    await_bytes(xb.at[:, pl.ds(0, (NX - 1) * tokens)], x_send)
    await_bytes(mx.at[pl.ds(0, (NX - 1) * tokens), :], m_send)
    await_bytes(edge.at[0], e_send.at[0])
    await_bytes(edge.at[1], e_send.at[1])
    await_bytes(gr.at[pl.ds(1, nz - 1)], z_send)


VM = pl.BlockSpec(memory_space=pltpu.VMEM)


def local(
    nz,
    ntp,
    out_grad,
    moe_input,
    route_weight,
    route_ids,
    gate_proj,
    up_proj,
    down_proj,
    out_proj,
    conv_out,
    gate_b,
    gate_c,
    value_v,
    conv_taps,
):
    tokens, chans = out_grad.shape
    ns = nz * NX
    cap = 4 * tokens // ns
    total = ns * cap
    width = chans * ntp
    dma = pltpu.SemaphoreType.DMA
    buf = pl.pallas_call(
        functools.partial(dispatch_kernel, nz),
        out_shape=jax.ShapeDtypeStruct((2, total, width), BF),
        in_specs=[VM] * 4,
        out_specs=VM,
        scratch_shapes=[
            pltpu.VMEM((2, total, chans), BF),
            pltpu.VMEM((8, 128), F32),
            dma,
            dma,
            dma((nz,)),
            dma,
            dma((3, nz)),
            dma((4,)),
        ],
        compiler_params=pltpu.CompilerParams(collective_id=0, has_side_effects=True),
        name="dispatch",
    )(out_grad, moe_input, route_weight, route_ids)
    xin, dyin = buf[0], buf[1]
    w_gate, w_up, w_down = gate_proj[0], up_proj[0], down_proj[0]
    gate = jnp.dot(xin, w_gate, preferred_element_type=F32)
    upval = jnp.dot(xin, w_up, preferred_element_type=F32)
    sig = jax.nn.sigmoid(gate)
    act = gate * sig
    hidden = (act * upval).astype(BF)
    dhid = jnp.dot(dyin, w_down.T, preferred_element_type=F32)
    dgate = (dhid * upval * (sig * (1.0 + gate * (1.0 - sig)))).astype(BF)
    dup = (dhid * act).astype(BF)
    part = (
        jnp.dot(dgate, w_gate.T, preferred_element_type=F32)
        + jnp.dot(dup, w_up.T, preferred_element_type=F32)
    ).astype(BF)
    grad_down = jnp.dot(hidden.T, dyin, preferred_element_type=F32).astype(BF)
    grad_gate = jnp.dot(xin.T, dgate, preferred_element_type=F32).astype(BF)
    grad_up = jnp.dot(xin.T, dup, preferred_element_type=F32).astype(BF)

    wide = chans // NX
    vm = pltpu.VMEM
    grad_out, grad_b, grad_c, grad_v = pl.pallas_call(
        functools.partial(tail_kernel, nz),
        out_shape=[
            jax.ShapeDtypeStruct((wide, chans), F32),
            jax.ShapeDtypeStruct((tokens, chans), BF),
            jax.ShapeDtypeStruct((tokens, chans), BF),
            jax.ShapeDtypeStruct((tokens, chans), BF),
        ],
        in_specs=[VM] * 9,
        out_specs=[VM] * 4,
        scratch_shapes=[
            vm((NY, total, chans), BF),
            vm((2, total, chans), BF),
            vm((total, chans), BF),
            vm((total, chans), BF),
            vm((total, chans), BF),
            vm((total, chans), BF),
            vm((total, chans), BF),
            vm((total, chans), BF),
            vm((tokens, chans), BF),
            vm((tokens, width), BF),
            vm((chans, tokens), BF),
            vm((wide, NX * tokens), BF),
            vm((ntp * wide, NX * tokens), BF),
            vm((tokens, chans), BF),
            vm((NX * tokens, chans), BF),
            vm((2, 16, chans), BF),
            vm((2, 16, chans), BF),
            vm((nz * wide, chans), BF),
            vm((nz, wide, chans), BF),
            dma((5,)),
            dma,
            dma((2,)),
            dma((3,)),
            dma((3, nz)),
            dma,
            dma,
            dma,
            dma((3, 2)),
            dma((4,)),
            dma,
            dma((3, 2)),
            dma((4,)),
            dma,
            dma,
            dma,
            dma,
            dma((2,)),
            dma((2,)),
            dma,
            dma,
        ],
        compiler_params=pltpu.CompilerParams(collective_id=1, has_side_effects=True),
        name="tail",
    )(part, out_grad, route_ids, out_proj, conv_out, gate_b, gate_c, value_v, conv_taps)
    return (grad_gate[None], grad_up[None], grad_down[None], grad_out, grad_b, grad_c, grad_v)


def solution(mesh):
    nz = mesh.shape["sp"] // NX
    ntp = mesh.shape["tp"]
    tok, tok_tp = P("sp", None), P("sp", "tp")
    return jax.shard_map(
        functools.partial(local, nz, ntp),
        mesh=mesh,
        in_specs=(
            tok_tp,
            tok_tp,
            tok,
            tok,
            P("sp", None, "tp"),
            P("sp", None, "tp"),
            P("sp", "tp", None),
            P(None, "tp"),
            tok_tp,
            tok_tp,
            tok_tp,
            tok_tp,
            P(None, "tp"),
        ),
        out_specs=(
            P("sp", None, "tp"),
            P("sp", None, "tp"),
            P("sp", "tp", None),
            tok_tp,
            tok_tp,
            tok_tp,
            tok_tp,
        ),
        check_vma=False,
    )
```

time: 292 us -> 125 us (0.43); the launches traced: 286 us -> 125 us
  waiting for transfers between devices: 145 us -> 0 us
  Pallas kernels: 0 us -> 99 us
  blocking collectives: 72.9 us -> 0 us
  starting transfers between devices: 15.1 us -> 0 us
  between operations: 14.2 us -> 0.71 us
  other arithmetic: 8.14 us -> 0 us
  local copies, waits for them, and re-layouts: 14.3 us -> 9.8 us
    pallas_call x0 -> x2, Pallas kernels: none -> 99 us  [the longest x1 54.3 us: local(): pl.pallas_call(functools.partial(tail_kernel, nz), out_shape=[jax.ShapeDt...]
    reduce_scatter x4 -> x0, waiting for transfers between devices: 97.7 us -> none  [own_block(): blocks = lax.psum_scatter(blocks, axes[k], scatter_dimension=0, tiled=True)]
    all_to_all x3 -> x0, blocking collectives: 72.9 us -> none  [the longest x1 30.2 us: summed_on_arrival(): lax.all_to_all(blocks, axis, split_axis=0, concat_axis=0, tiled=True)]
    all_gather x1 -> x0, waiting for transfers between devices: 36.7 us -> none  [in_one_piece(): lax.all_gather(both, axis, axis=dim, tiled=True)]
    all_to_all x1 -> x0, waiting for transfers between devices: 10.5 us -> none  [local(): lax.all_to_all(summed.reshape(n_experts, capacity, local_cols), SP, split...]
    all_to_all x1 -> x0, starting transfers between devices: 9.67 us -> none  [local(): lax.all_to_all(summed.reshape(n_experts, capacity, local_cols), SP, split...]
    unnamed x44 -> x14, local copies, waits for them, and re-layouts: 3.7 us -> 9.8 us
    ppermute x2 -> x0, starting transfers between devices: 5.27 us -> none  [the longest x1 3.99 us: with_halo(): lax.ppermute(lax.slice_in_dim(block, block.shape[dim] - width, None, axis...]
  transfers between devices with their start and end apart: 8 -> 0, of which waited for: 6 -> 0; matrix products, arithmetic and copies ran while one was open for 4% -> 0% of each run, Pallas kernels for 0% -> 0%
where the time goes in v1:
time: 125 us
  Pallas kernels  99 us (79%)
  matrix products  15 us (12%)
  local copies, waits for them, and re-layouts  9.8 us (8%)
    pallas_call x1, Pallas kernels, local(): pl.pallas_call(functools.partial(tail_kernel, nz), out_shape=[jax.ShapeDt...  54.3 us
    pallas_call x1, Pallas kernels, local(): pl.pallas_call(functools.partial(dispatch_kernel, nz), out_shape=jax.Shap...  44.7 us
    unnamed x14, local copies, waits for them, and re-layouts  9.8 us
    dot_general x1, matrix products, local(): jnp.dot(dup, w_up.T, preferred_element_type=F32)  2.71 us
    dot_general x1, matrix products, local(): gate = jnp.dot(xin, w_gate, preferred_element_type=F32)  2.68 us

profile of v1, /device:TPU:1, one launch (start us, length us, event | category | flops | bytes accessed | tf_op | source)
XLA Modules:
  0.0 124.6 jit_solution(1242439530871007981)
XLA Ops:
  0.6 0.0 copy-start
  0.6 1.5 %copy.21.ids_ref = s32[128,2]{1,0:T(8,128)} copy(s32[128,2]{0,1:T(2,128)} %param.16) | data formatting | bytes 2048 | tf_op args[3]
  2.2 1.4 %copy.20.rw_ref = f32[128,2]{1,0:T(8,128)} copy(f32[128,2]{0,1:T(2,128)} %param.15) | data formatting | bytes 2048 | tf_op args[2]
  3.6 44.7 %dispatch.1 = bf16[2,512,2048]{2,1,0:T(8,128)(2,1)} custom-call(bf16[128,256]{1,0:T(8,128)(2,1)} %og_ref.3, bf16[128,256]{1,0:T(8,128)(2,1)} %x_ref.1, f32[128,2]{1,0:T(8,128)} %copy.20.rw_ref, s32[128,2]{1,0:T(8,128)} %copy.21.ids_ref), custom_call_target="tpu_custom_call" | custom-call | tf_op jit(solution)/shard_map/dispatch/pallas_call | solution.py:489
  48.3 0.0 copy-done
  48.3 0.0 copy-start.1
  48.3 0.0 copy-start.2
  48.3 2.7 %fusion.8 = f32[512,352]{0,1:T(8,128)S(1)} fusion(bf16[1,2048,352]{1,2,0:T(8,128)(2,1)S(1)} %copy-done, bf16[2,512,2048]{2,1,0:T(8,128)(2,1)} %dispatch.1), kind=kOutput, calls=%fused_computation.12 | convolution fusion | flops 738197504 | bytes 4259840 | tf_op jit(solution)/shard_map/dot_general | solution.py:509
  51.0 0.1 copy-done.1
  51.1 0.4 copy-done.2
  51.6 0.0 copy-start.3
  51.6 0.9 fusion.10
  52.5 0.4 copy-done.3
  52.9 1.2 multiply_convert_fusion.1
  54.2 2.1 %fusion = bf16[1,352,2048]{2,1,0:T(8,128)(2,1)} fusion(bf16[2,512,2048]{2,1,0:T(8,128)(2,1)S(1)} %copy-done.1, f32[512,352]{0,1:T(8,128)S(1)} %fusion.10, f32[512,352]{0,1:T(8,128)S(1)} %fusion.8), kind=kOutput, calls=%fused_computation.4 | convolution fusion | flops 739999744 | bytes 4980736 | tf_op jit(solution)/shard_map/dot_general | solution.py:521
  56.2 2.1 %fusion.2 = bf16[1,2048,352]{1,2,0:T(8,128)(2,1)} fusion(bf16[512,352]{0,1:T(8,128)(2,1)S(1)} %get-tuple-element.15, bf16[2,512,2048]{2,1,0:T(8,128)(2,1)S(1)} %copy-done.1), kind=kOutput, calls=%fused_computation.6 | convolution fusion | flops 738918400 | bytes 3899392 | tf_op jit(solution)/shard_map/dot_general | solution.py:523
  58.3 2.1 %fusion.1 = bf16[1,2048,352]{1,2,0:T(8,128)(2,1)} fusion(bf16[512,352]{0,1:T(8,128)(2,1)S(1)} %get-tuple-element.16, bf16[2,512,2048]{2,1,0:T(8,128)(2,1)S(1)} %copy-done.1), kind=kOutput, calls=%fused_computation.5 | convolution fusion | flops 738918400 | bytes 3899392 | tf_op jit(solution)/shard_map/dot_general | solution.py:522
  60.3 1.3 %fusion.14 = f32[512,2048]{1,0:T(8,128)S(1)} fusion(bf16[512,352]{0,1:T(8,128)(2,1)S(1)} %get-tuple-element.16, bf16[1,2048,352]{1,2,0:T(8,128)(2,1)S(1)} %copy-done), kind=kOutput, calls=%fused_computation.18 | convolution fusion | flops 738197504 | bytes 5996544 | tf_op jit(solution)/shard_map/dot_general | solution.py:518
  61.6 2.7 %add_convert_fusion.part_ref = bf16[512,2048]{1,0:T(8,128)(2,1)} fusion(f32[512,2048]{1,0:T(8,128)S(1)} %fusion.14, bf16[512,352]{0,1:T(8,128)(2,1)S(1)} %get-tuple-element.15, bf16[1,2048,352]{1,2,0:T(8,128)(2,1)S(1)} %copy-done.2), kind=kOutput, calls=%fused_computation | convolution fusion | flops 740294656 | bytes 8093696 | tf_op jit(solution)/shard_map/dot_general | solution.py:519
  64.3 54.3 %tail.1 = (f32[64,256]{1,0:T(8,128)}, bf16[128,256]{1,0:T(8,128)(2,1)}, bf16[128,256]{1,0:T(8,128)(2,1)}, bf16[128,256]{1,0:T(8,128)(2,1)}) custom-call(bf16[512,2048]{1,0:T(8,128)(2,1)} %add_convert_fusion.part_ref, bf16[128,256]{1,0:T(8,128)(2,1)} %og_ref.3, s32[128,2]{1,0:T(8,128)} %copy.21.ids_ref, bf16[2048,256]{1,0:T(8,128)(2,1)} %out_proj_ref.1, ...), custom_call_target="tpu_custom_call" | custom-call | tf_op jit(solution)/shard_map/tail/pallas_call | solution.py:527
  118.7 1.5 %copy.27 = f32[64,256]{1,0:T(8,128)} copy(f32[64,256]{1,0:T(8,128)} %get-tuple-element.27) | data formatting | bytes 131072
  120.1 1.5 %copy.28 = bf16[128,256]{1,0:T(8,128)(2,1)} copy(bf16[128,256]{1,0:T(8,128)(2,1)} %get-tuple-element.28) | data formatting | bytes 131072
  121.6 1.5 %copy.29 = bf16[128,256]{1,0:T(8,128)(2,1)} copy(bf16[128,256]{1,0:T(8,128)(2,1)} %get-tuple-element.29) | data formatting | bytes 131072
  123.1 1.5 %copy.30 = bf16[128,256]{1,0:T(8,128)(2,1)} copy(bf16[128,256]{1,0:T(8,128)(2,1)} %get-tuple-element.30) | data formatting | bytes 131072
Async XLA Ops:
  0.6 47.7 %copy-start = (bf16[1,2048,352]{1,2,0:T(8,128)(2,1)S(1)}, bf16[1,2048,352]{1,2,0:T(8,128)(2,1)}, u32[]{:S(2)}) copy-start(bf16[1,2048,352]{1,2,0:T(8,128)(2,1)} %param.17) | copy-start | bytes 4325380
  48.3 2.8 %copy-start.1 = (bf16[2,512,2048]{2,1,0:T(8,128)(2,1)S(1)}, bf16[2,512,2048]{2,1,0:T(8,128)(2,1)}, u32[]{:S(2)}) copy-start(bf16[2,512,2048]{2,1,0:T(8,128)(2,1)} %dispatch.1) | copy-start | bytes 12582916
  48.3 3.3 %copy-start.2 = (bf16[1,2048,352]{1,2,0:T(8,128)(2,1)S(1)}, bf16[1,2048,352]{1,2,0:T(8,128)(2,1)}, u32[]{:S(2)}) copy-start(bf16[1,2048,352]{1,2,0:T(8,128)(2,1)} %param.18) | copy-start | bytes 4325380
  51.6 1.4 %copy-start.3 = (bf16[1,352,2048]{2,1,0:T(8,128)(2,1)S(1)}, bf16[1,352,2048]{2,1,0:T(8,128)(2,1)}, u32[]{:S(2)}) copy-start(bf16[1,352,2048]{2,1,0:T(8,128)(2,1)} %param.19) | copy-start | bytes 4325380

commit v2 on v1

v2 whole, which is shorter than its diff:
```python
import functools

import jax
import jax.numpy as jnp
from jax import lax
from jax.experimental import pallas as pl
from jax.experimental.pallas import tpu as pltpu
from jax.sharding import PartitionSpec as P

MESH = pl.DeviceIdType.MESH
NX = 4
NY = 4
BF = jnp.bfloat16
F32 = jnp.float32


def block_order(nz):
    order = [0]
    for d in range(1, nz // 2 + 1):
        order.append(d)
        if nz - d != d:
            order.append(nz - d)
    return order[:nz]


class Place:
    def __init__(self, nz):
        self.nz = nz
        self.sp = lax.axis_index("sp")
        self.tp = lax.axis_index("tp")
        self.z = lax.div(self.sp, NX)
        self.x = lax.rem(self.sp, NX)
        self.y = lax.div(self.tp, 2)
        self.c = lax.rem(self.tp, 2)

    def over_sp(self, dz, dx):
        z = lax.rem(self.z + dz, self.nz)
        x = lax.rem(self.x + dx, NX)
        return (z * NX + x, self.tp)

    def over_y(self, dy):
        return (self.sp, lax.rem(self.y + dy + NY, NY) * 2 + self.c)

    def other(self):
        return (self.sp, self.y * 2 + 1 - self.c)

    def origin(self, dy, flip):
        y = lax.rem(self.y + dy + NY, NY)
        c = 1 - self.c if flip else self.c
        return y * 2 + c


def greet(here):
    barrier = pltpu.get_barrier_semaphore()
    peers = [here.over_sp(dz, dx) for dz in range(here.nz) for dx in range(NX) if dz or dx]
    peers += [here.other(), here.over_y(1), here.over_y(-1)]
    for peer in peers:
        pl.semaphore_signal(barrier, inc=1, device_id=peer, device_id_type=MESH)
    return barrier, len(peers)


def send(src, dst, send_sem, recv_sem, peer):
    copy = pltpu.make_async_remote_copy(
        src_ref=src,
        dst_ref=dst,
        send_sem=send_sem,
        recv_sem=recv_sem,
        device_id=peer,
        device_id_type=MESH,
    )
    copy.start()


def await_bytes(ref, sem):
    pltpu.make_async_copy(ref, ref, sem).wait()


class Gather:
    def __init__(self, here, chunk, send_sem, near, far, group=lambda h: 0):
        self.here, self.chunk, self.send_sem = here, chunk, send_sem
        self.near, self.far, self.group = near, far, group

    def _send(self, origin, h, peer, recv_sem):
        ref = self.chunk(origin, h)
        send(ref, ref, self.send_sem, recv_sem, peer)

    def start(self, h):
        here = self.here
        mine = here.origin(0, False)
        self._send(mine, h, here.over_y(1), self.near.at[0, h])
        self._send(mine, h, here.over_y(-1), self.near.at[1, h])
        self._send(mine, h, here.other(), self.far.at[0, self.group(h)])

    def forward(self, h):
        here = self.here
        low, high = here.origin(-1, False), here.origin(1, False)
        await_bytes(self.chunk(low, h), self.near.at[0, h])
        if h % 2 == 0:
            self._send(low, h, here.over_y(1), self.near.at[2, h])
        self._send(low, h, here.other(), self.far.at[1, self.group(h)])
        await_bytes(self.chunk(high, h), self.near.at[1, h])
        if h % 2 == 1:
            self._send(high, h, here.over_y(-1), self.near.at[2, h])
        self._send(high, h, here.other(), self.far.at[2, self.group(h)])

    def last(self, h):
        here = self.here
        across = here.origin(2, False)
        await_bytes(self.chunk(across, h), self.near.at[2, h])
        self._send(across, h, here.other(), self.far.at[3, self.group(h)])

    def finish(self, whole, g=0):
        here = self.here
        for k, dy in enumerate((0, -1, 1, 2)):
            await_bytes(whole(here.origin(dy, True)), self.far.at[k, g])


def slots_of(ids, here, total):
    tokens = ids.shape[0]
    lanes = lax.broadcasted_iota(jnp.int32, (tokens, 128), 1)
    named = [(lanes == ids[:, k : k + 1]).astype(F32) for k in range(2)]
    rows = lax.broadcasted_iota(jnp.int32, (tokens, tokens), 0)
    cols = lax.broadcasted_iota(jnp.int32, (tokens, tokens), 1)
    earlier = (cols < rows).astype(F32).astype(BF)
    before = jnp.dot(earlier, (named[0] + named[1]).astype(BF), preferred_element_type=F32)
    cap = total // (here.nz * NX)
    out = []
    for k in range(2):
        slot = jnp.sum(before * named[k], axis=1, keepdims=True)
        e = ids[:, k : k + 1]
        dz = ((e // NX if NX not in (1, 2, 4) else (e >> (NX.bit_length() - 1))) - here.z) & (here.nz - 1)
        dx = ((e & (NX - 1)) - here.x) & (NX - 1)
        out.append(((dz * NX + dx) * cap).astype(F32) + slot)
    return out


def nt(a, b):
    return lax.dot_general(a, b, (((1,), (1,)), ((), ())), preferred_element_type=F32)


def step_kernel(
    nz,
    og_ref,
    x_ref,
    rw_ref,
    ids_ref,
    conv_ref,
    gb_ref,
    gc_ref,
    vv_ref,
    taps_ref,
    wg_hbm,
    wu_hbm,
    wd_hbm,
    op_hbm,
    go_ref,
    gradb_ref,
    gradc_ref,
    gradv_ref,
    rows_hbm,
    dt_hbm,
    sbuf,
    buf,
    wcat,
    wd,
    out_proj,
    dcat,
    dt,
    part,
    pr,
    sb,
    ra,
    rb,
    sc,
    rc,
    fin,
    ret,
    pick,
    dh,
    dhall,
    dht,
    xall,
    mixed,
    mx,
    edge,
    halo,
    gpart,
    gr,
    w_sem,
    own_sem,
    a_send,
    a_recv,
    g_send,
    g_near,
    g_far,
    pair_send,
    pair_recv,
    rs_send,
    rs_recv,
    sp_send,
    sp_recv,
    dh_send,
    dh_near,
    dh_far,
    xb_send,
    xb_near,
    xb_far,
    x_send,
    x_recv,
    m_send,
    m_recv,
    e_send,
    e_recv,
    z_send,
    z_recv,
):
    here = Place(nz)
    barrier, peers = greet(here)
    total, chans = sbuf.shape[1:]
    cap = total // (nz * NX)
    tokens = og_ref.shape[0]
    hid, padded = wg_hbm.shape[0], wd.shape[0]
    order = block_order(nz)
    at = {d: p for p, d in enumerate(order)}
    rows = NX * cap
    half = total // 2
    hb = nz // 2

    loads = [
        pltpu.make_async_copy(wg_hbm, wcat.at[0:hid, :], w_sem.at[0]),
        pltpu.make_async_copy(wu_hbm, wcat.at[padded : padded + hid, :], w_sem.at[1]),
        pltpu.make_async_copy(wd_hbm, wd.at[0:hid, :], w_sem.at[2]),
        pltpu.make_async_copy(op_hbm, out_proj, w_sem.at[3]),
    ]
    for load in loads:
        load.start()

    ids = ids_ref[...].astype(F32).T.astype(jnp.int32)
    rw = rw_ref[...].T
    slots = slots_of(ids, here, total)
    srow = lax.broadcasted_iota(jnp.int32, (total, tokens), 0).astype(F32)
    places = []
    for k in range(2):
        wide = jnp.broadcast_to(slots[k], (tokens, tokens)).T
        places.append((srow == wide[0:1, :]).astype(F32))
    both = (places[0] + places[1]).astype(BF)
    sbuf[0] = jnp.dot(both, x_ref[...], preferred_element_type=F32).astype(BF)
    og = og_ref[...].astype(F32)
    dy = None
    for k in range(2):
        weighted = (rw[:, k : k + 1] * og).astype(BF)
        term = jnp.dot(places[k].astype(BF), weighted, preferred_element_type=F32)
        dy = term if dy is None else dy + term
    sbuf[1] = dy.astype(BF)
    scol = lax.broadcasted_iota(jnp.int32, (tokens, total), 1).astype(F32)
    pick[...] = ((scol == slots[0]).astype(F32) + (scol == slots[1]).astype(F32)).astype(BF)
    mixed[...] = (gb_ref[...].astype(F32) * conv_ref[...].astype(F32)).astype(BF)
    wcat[hid:padded, :] = jnp.zeros((padded - hid, wcat.shape[1]), BF)
    wcat[padded + hid :, :] = jnp.zeros((padded - hid, wcat.shape[1]), BF)
    wd[hid:, :] = jnp.zeros((padded - hid, wcat.shape[1]), BF)

    def cols(origin):
        return pl.ds(pl.multiple_of(origin * chans, chans), chans)

    column = cols(here.tp)
    pl.semaphore_wait(barrier, peers)
    own = pltpu.make_async_copy(sbuf.at[:, 0:cap, :], buf.at[:, 0:cap, column], own_sem.at[5])
    own.start()
    for dz in order:
        for dx in range(NX):
            if dz or dx:
                r = (dz * NX + dx) * cap
                p = at[(-dz) % nz]
                t = p * rows + ((-dx) % NX) * cap
                send(
                    sbuf.at[:, pl.ds(r, cap), :],
                    buf.at[:, pl.ds(t, cap), column],
                    a_send,
                    a_recv.at[p],
                    here.over_sp(dz, dx),
                )
    mrow = pl.ds(pl.multiple_of(here.x * tokens, tokens), tokens)
    own_mixed = pltpu.make_async_copy(mixed, mx.at[mrow, :], own_sem.at[0])
    own_mixed.start()

    def chunk(origin, h):
        return buf.at[:, pl.ds(h * rows, rows), cols(origin)]

    gather = Gather(here, chunk, g_send, g_near, g_far, lambda h: h // hb)

    def experts(r0, n):
        r = pl.ds(r0, n)
        gu = nt(buf[0, r, :], wcat[...])
        dhid = nt(buf[1, r, :], wd[...])
        gate, upval = gu[:, :padded], gu[:, padded:]
        sig = jax.nn.sigmoid(gate)
        act = gate * sig
        dcat[r, 0:padded] = (dhid * upval * (sig * (1.0 + gate * (1.0 - sig)))).astype(BF)
        dcat[r, padded : 2 * padded] = (dhid * act).astype(BF)
        dcat[r, 2 * padded :] = (act * upval).astype(BF)

    def whole(k):
        return lambda origin: buf.at[:, pl.ds(k * half, half), cols(origin)]

    def early(step):
        if step == 0:
            gather.finish(whole(0), 0)
            for load in loads[:3]:
                load.wait()
        n = half // EARLY
        if step < EARLY:
            experts(step * n, n)

    done = 0
    for p in range(nz + LAST):
        if p < nz:
            if p == 0:
                own.wait()
                await_bytes(buf.at[:, cap:rows, column], a_recv.at[0])
            else:
                await_bytes(buf.at[:, pl.ds(p * rows, rows), column], a_recv.at[p])
            gather.start(p)
        if p == nz - 1:
            for dx in range(1, NX):
                send(mixed, mx.at[mrow, :], m_send, m_recv, here.over_sp(0, dx))
        if 0 <= p - FORWARD < nz:
            gather.forward(p - FORWARD)
        if 0 <= p - LAST < nz:
            gather.last(p - LAST)
        if p >= hb + LAST and done < EARLY:
            early(done)
            done += 1
    while done < EARLY:
        early(done)
        done += 1
    gather.finish(whole(1), 1)
    keep_rows = pltpu.make_async_copy(buf, rows_hbm, own_sem.at[6])
    keep_rows.start()
    experts(half, half)

    def spread(k):
        r = pl.ds(k * half, half)
        d = dcat[r, 0 : 2 * padded]
        step = 2 * chans
        for n in range(NY):
            c = pl.ds(n * step, step)
            part[r, c] = jnp.dot(d, wcat[:, c], preferred_element_type=F32).astype(BF)
        for y in range(NY):
            send(
                part.at[r, cols(2 * y + 1 - here.c)],
                pr.at[y, r, :],
                pair_send,
                pair_recv.at[k],
                here.other(),
            )

    spread(1)
    spread(0)

    def pair(p, dy):
        y = lax.rem(here.y + dy + NY, NY)
        r = pl.ds(p * rows, rows)
        return part[r, cols(2 * y + here.c)].astype(F32) + pr[y, r, :].astype(F32)

    def stage_a(p):
        way = 1 if p % 2 == 0 else -1
        r = pl.ds(p * rows, rows)
        if p == nz - 1:
            await_bytes(pr.at[:, pl.ds(half, half), :], pair_recv.at[1])
        if p == hb - 1:
            await_bytes(pr.at[:, pl.ds(0, half), :], pair_recv.at[0])
        sb[0, r, :] = pair(p, 2).astype(BF)
        send(sb.at[0, r, :], ra.at[r, :], rs_send.at[0], rs_recv.at[0, p], here.over_y(way))
        sb[1, r, :] = pair(p, -way).astype(BF)
        send(sb.at[1, r, :], rb.at[r, :], rs_send.at[1], rs_recv.at[1, p], here.over_y(-way))

    def stage_b(p):
        way = 1 if p % 2 == 0 else -1
        r = pl.ds(p * rows, rows)
        await_bytes(ra.at[r, :], rs_recv.at[0, p])
        sc[r, :] = (pair(p, way) + ra[r, :].astype(F32)).astype(BF)
        send(sc.at[r, :], rc.at[r, :], rs_send.at[2], rs_recv.at[2, p], here.over_y(way))

    def stage_c(p):
        r = pl.ds(p * rows, rows)
        await_bytes(rb.at[r, :], rs_recv.at[1, p])
        await_bytes(rc.at[r, :], rs_recv.at[2, p])
        fin[r, :] = (pair(p, 0) + rb[r, :].astype(F32) + rc[r, :].astype(F32)).astype(BF)
        dz = order[p]
        for dx in range(NX):
            src = fin.at[pl.ds(p * rows + dx * cap, cap), :]
            t = (((-dz) % nz) * NX + (-dx) % NX) * cap
            dst = ret.at[pl.ds(t, cap), :]
            if dz or dx:
                send(src, dst, sp_send, sp_recv, here.over_sp(dz, dx))

    for s in range(nz + STAGE_C):
        if s < nz:
            stage_a(nz - 1 - s)
        if 0 <= s - STAGE_B < nz:
            stage_b(nz - 1 - (s - STAGE_B))
        if 0 <= s - STAGE_C < nz:
            stage_c(nz - 1 - (s - STAGE_C))
    ret[0:cap, :] = fin[0:cap, :]

    slab = 3 * padded // 9

    def turn(k):
        dt[k * slab : (k + 1) * slab, :] = dcat[:, k * slab : (k + 1) * slab].astype(F32).T.astype(BF)

    for k in range(3):
        turn(k)
    await_bytes(ret.at[pl.ds(cap, total - cap), :], sp_recv)

    moe = jnp.dot(pick[...], ret[...], preferred_element_type=F32)
    grad_h = og_ref[...].astype(F32) + moe
    dht[...] = grad_h.T.astype(BF)
    dh[...] = grad_h.astype(BF)

    wide = chans // NX
    tcol = pl.ds(pl.multiple_of(here.x * tokens, tokens), tokens)

    def orows(origin, h=0, n=1):
        size = wide // n
        return pl.ds(pl.multiple_of(origin * wide + h * size, size), size)

    for dx in range(1, NX):
        to = lax.rem(here.x + dx, NX)
        send(
            dht.at[orows(to), :],
            xall.at[orows(here.tp), tcol],
            x_send,
            x_recv,
            here.over_sp(0, dx),
        )
    own_x = pltpu.make_async_copy(dht.at[orows(here.x), :], xall.at[orows(here.tp), tcol], own_sem.at[1])
    own_x.start()
    own_dh = pltpu.make_async_copy(dh, dhall.at[:, column], own_sem.at[2])
    own_dh.start()
    own_dh.wait()
    ht = tokens // 2
    dh_gather = Gather(here, lambda o, h: dhall.at[pl.ds(h * ht, ht), cols(o)], dh_send, dh_near, dh_far)
    xb_gather = Gather(here, lambda o, h: xall.at[orows(o, h, 2), :], xb_send, xb_near, xb_far)
    dh_gather.start(0)
    dh_gather.start(1)
    for k in range(3, 6):
        turn(k)
    own_x.wait()
    await_bytes(xall.at[pl.ds(0, wide), pl.ds(0, (NX - 1) * tokens)], x_recv)
    xb_gather.start(0)
    xb_gather.start(1)
    for h in range(2):
        dh_gather.forward(h)
    for h in range(2):
        dh_gather.last(h)
    for k in range(6, 9):
        turn(k)
    keep_dt = pltpu.make_async_copy(dt, dt_hbm, own_sem.at[3])
    keep_dt.start()
    for h in range(2):
        xb_gather.forward(h)
    dh_gather.finish(lambda o: dhall.at[:, cols(o)])
    loads[3].wait()
    grad_z = jnp.dot(dhall[...], out_proj[...], preferred_element_type=F32)
    dconv = (grad_z * gb_ref[...].astype(F32)).astype(BF)
    edge[0, :, :] = dconv[0:16, :]
    edge[1, :, :] = dconv[tokens - 16 :, :]
    last_sp = nz * NX
    before = (lax.rem(here.sp + last_sp - 1, last_sp), here.tp)
    after = (lax.rem(here.sp + 1, last_sp), here.tp)
    for h in range(2):
        xb_gather.last(h)
    send(edge.at[0], halo.at[1], e_send.at[0], e_recv.at[1], before)
    send(edge.at[1], halo.at[0], e_send.at[1], e_recv.at[0], after)
    own_mixed.wait()
    await_bytes(mx.at[pl.ds(0, (NX - 1) * tokens), :], m_recv)
    xb_gather.finish(lambda o: xall.at[orows(o), :])
    gpart[...] = jnp.dot(xall[...], mx[...], preferred_element_type=F32).astype(BF)
    for dz in range(1, nz):
        to = lax.rem(here.z + dz, nz)
        send(gpart.at[orows(to), :], gr.at[dz], z_send, z_recv, here.over_sp(dz, 0))
    own_g = pltpu.make_async_copy(gpart.at[orows(here.z), :], gr.at[0], own_sem.at[4])
    own_g.start()

    gradb_ref[...] = (grad_z * conv_ref[...].astype(F32)).astype(BF)
    await_bytes(halo.at[0], e_recv.at[0])
    await_bytes(halo.at[1], e_recv.at[1])
    dconv = dconv.astype(F32)
    row = lax.broadcasted_iota(jnp.int32, dconv.shape, 0)
    low = halo[0].astype(F32)[15:16, :] * (here.sp > 0).astype(F32)
    high = halo[1].astype(F32)[0:1, :] * (here.sp < last_sp - 1).astype(F32)
    prev = jnp.where(row == 0, low, pltpu.roll(dconv, 1, 0))
    nxt = jnp.where(row == tokens - 1, high, pltpu.roll(dconv, tokens - 1, 0))
    grad_u = taps_ref[0:1, :] * nxt + taps_ref[1:2, :] * dconv + taps_ref[2:3, :] * prev
    gradc_ref[...] = (grad_u * vv_ref[...].astype(F32)).astype(BF)
    gradv_ref[...] = (grad_u * gc_ref[...].astype(F32)).astype(BF)

    others = 2 * NY - 1
    await_bytes(sbuf.at[:, pl.ds(0, total - cap), :], a_send)
    await_bytes(buf.at[:, pl.ds(0, total - total // (2 * NY)), :], g_send)
    await_bytes(pr, pair_send)
    for k in range(3):
        await_bytes(ra, rs_send.at[k])
    await_bytes(ret.at[pl.ds(cap, total - cap), :], sp_send)
    await_bytes(dhall.at[:, pl.ds(0, others * chans)], dh_send)
    await_bytes(xall.at[pl.ds(0, others * wide), :], xb_send)
    await_bytes(xall.at[pl.ds(0, wide), pl.ds(0, (NX - 1) * tokens)], x_send)
    await_bytes(mx.at[pl.ds(0, (NX - 1) * tokens), :], m_send)
    await_bytes(edge.at[0], e_send.at[0])
    await_bytes(edge.at[1], e_send.at[1])
    keep_rows.wait()
    keep_dt.wait()

    own_g.wait()
    await_bytes(gr.at[pl.ds(1, nz - 1)], z_recv)
    summed = gr[0].astype(F32)
    for k in range(1, nz):
        summed = summed + gr[k].astype(F32)
    go_ref[...] = summed
    await_bytes(gr.at[pl.ds(1, nz - 1)], z_send)


def grads_kernel(rows_ref, dt_ref, go, gb, gc, gv, gate_ref, up_ref, down_ref, go_ref, gb_ref, gc_ref, gv_ref):
    hid, padded = gate_ref.shape[0], dt_ref.shape[0] // 3
    x, dy = rows_ref[0], rows_ref[1]
    both = jnp.dot(dt_ref[0 : 2 * padded, :], x, preferred_element_type=F32)
    gate_ref[...] = both[0:hid, :].astype(BF)
    up_ref[...] = both[padded : padded + hid, :].astype(BF)
    down_ref[...] = jnp.dot(dt_ref[2 * padded :, :], dy, preferred_element_type=F32)[0:hid, :].astype(BF)

    @pl.when(pl.program_id(0) == 0)
    def _():
        go_ref[...] = go[...]
        gb_ref[...] = gb[...]
        gc_ref[...] = gc[...]
        gv_ref[...] = gv[...]


VM = pl.BlockSpec(memory_space=pltpu.VMEM)
ANY = pl.BlockSpec(memory_space=pl.ANY)
FORWARD, LAST = 2, 4
STAGE_B, STAGE_C = 2, 4
EARLY = 2


def local(
    nz,
    ntp,
    out_grad,
    moe_input,
    route_weight,
    route_ids,
    gate_proj,
    up_proj,
    down_proj,
    out_proj,
    conv_out,
    gate_b,
    gate_c,
    value_v,
    conv_taps,
):
    tokens, chans = out_grad.shape
    ns = nz * NX
    cap = 4 * tokens // ns
    total = ns * cap
    width = chans * ntp
    hid = gate_proj.shape[2]
    padded = -(-hid // 128) * 128
    wide = chans // NX
    dma = pltpu.SemaphoreType.DMA

    def vm(*shape):
        return pltpu.VMEM(shape, BF)

    small = [
        jax.ShapeDtypeStruct((wide, chans), F32),
        jax.ShapeDtypeStruct((tokens, chans), BF),
        jax.ShapeDtypeStruct((tokens, chans), BF),
        jax.ShapeDtypeStruct((tokens, chans), BF),
    ]
    *results, kept_rows, kept_dt = pl.pallas_call(
        functools.partial(step_kernel, nz),
        out_shape=[
            *small,
            jax.ShapeDtypeStruct((2, total, width), BF),
            jax.ShapeDtypeStruct((3 * padded, total), BF),
        ],
        in_specs=[VM] * 9 + [ANY] * 4,
        out_specs=[VM] * 4 + [ANY] * 2,
        scratch_shapes=[
            vm(2, total, chans),
            vm(2, total, width),
            vm(2 * padded, width),
            vm(padded, width),
            vm(width, chans),
            vm(total, 3 * padded),
            vm(3 * padded, total),
            vm(total, width),
            vm(NY, total, chans),
            vm(2, total, chans),
            vm(total, chans),
            vm(total, chans),
            vm(total, chans),
            vm(total, chans),
            vm(total, chans),
            vm(total, chans),
            vm(tokens, total),
            vm(tokens, chans),
            vm(tokens, width),
            vm(chans, tokens),
            vm(ntp * wide, NX * tokens),
            vm(tokens, chans),
            vm(NX * tokens, chans),
            vm(2, 16, chans),
            vm(2, 16, chans),
            vm(nz * wide, chans),
            vm(nz, wide, chans),
            dma((4,)),
            dma((7,)),
            dma,
            dma((nz,)),
            dma,
            dma((3, nz)),
            dma((4, 2)),
            dma,
            dma((2,)),
            dma((3,)),
            dma((3, nz)),
            dma,
            dma,
            dma,
            dma((3, 2)),
            dma((4, 1)),
            dma,
            dma((3, 2)),
            dma((4, 1)),
            dma,
            dma,
            dma,
            dma,
            dma((2,)),
            dma((2,)),
            dma,
            dma,
        ],
        compiler_params=pltpu.CompilerParams(
            collective_id=0, has_side_effects=True, vmem_limit_bytes=60 * 1024 * 1024
        ),
        name="step",
    )(
        out_grad,
        moe_input,
        route_weight.T,
        route_ids.T,
        conv_out,
        gate_b,
        gate_c,
        value_v,
        conv_taps,
        gate_proj[0].T,
        up_proj[0].T,
        down_proj[0],
        out_proj,
    )

    step = width // 8

    def held(shape):
        return pl.BlockSpec(shape, lambda i: (0, 0))

    weights = pl.BlockSpec((hid, step), lambda i: (0, i))
    grad_gate, grad_up, grad_down, grad_out, grad_b, grad_c, grad_v = pl.pallas_call(
        grads_kernel,
        grid=(width // step,),
        out_shape=[jax.ShapeDtypeStruct((hid, width), BF)] * 3 + small,
        in_specs=[pl.BlockSpec((2, total, step), lambda i: (0, 0, i)), held(kept_dt.shape)]
        + [held(s.shape) for s in small],
        out_specs=[weights] * 3 + [held(s.shape) for s in small],
        name="grads",
    )(kept_rows, kept_dt, *results)
    return (grad_gate.T[None], grad_up.T[None], grad_down[None], grad_out, grad_b, grad_c, grad_v)


def solution(mesh):
    nz = mesh.shape["sp"] // NX
    ntp = mesh.shape["tp"]
    tok, tok_tp = P("sp", None), P("sp", "tp")
    return jax.shard_map(
        functools.partial(local, nz, ntp),
        mesh=mesh,
        in_specs=(
            tok_tp,
            tok_tp,
            tok,
            tok,
            P("sp", None, "tp"),
            P("sp", None, "tp"),
            P("sp", "tp", None),
            P(None, "tp"),
            tok_tp,
            tok_tp,
            tok_tp,
            tok_tp,
            P(None, "tp"),
        ),
        out_specs=(
            P("sp", None, "tp"),
            P("sp", None, "tp"),
            P("sp", "tp", None),
            tok_tp,
            tok_tp,
            tok_tp,
            tok_tp,
        ),
        check_vma=False,
    )
```

time: 125 us -> 95.8 us (0.77)
  matrix products: 15 us -> 0 us
  local copies, waits for them, and re-layouts: 9.8 us -> 0 us
  Pallas kernels: 99 us -> 94.8 us
    dot_general x8 -> x0, matrix products: 15 us -> none  [the longest x1 2.71 us: local(): jnp.dot(dup, w_up.T, preferred_element_type=F32)]
    unnamed x14 -> x0, local copies, waits for them, and re-layouts: 9.8 us -> none
    pallas_call x2, Pallas kernels: 99 us -> 94.8 us  [the longest x1 86.1 us: local(): pl.pallas_call(functools.partial(step_kernel, nz), out_shape=[*small, jax...]
where the time goes in v2:
time: 95.8 us; the launch traced here: 95.5 us
  Pallas kernels  94.8 us (99%)
    pallas_call x1, Pallas kernels, local(): pl.pallas_call(functools.partial(step_kernel, nz), out_shape=[*small, jax...  86.1 us
    pallas_call x1, Pallas kernels, local(): pl.pallas_call(grads_kernel, grid=(width // step,), out_shape=[jax.ShapeD...  8.73 us

profile of v2, /device:TPU:1, one launch (start us, length us, event | category | flops | bytes accessed | tf_op | source)
XLA Modules:
  0.0 95.5 jit_solution(11391890207845187721)
XLA Ops:
  0.6 86.1 %step.1 = (f32[64,256]{1,0:T(8,128)}, bf16[128,256]{1,0:T(8,128)(2,1)}, bf16[128,256]{1,0:T(8,128)(2,1)}, bf16[128,256]{1,0:T(8,128)(2,1)}, bf16[2,512,2048]{2,1,0:T(8,128)(2,1)}, /*index=5*/bf16[1152,512]{1,0:T(8,128)(2,1)}) custom-call(bf16[128,256]{1,0:T(8,128)(2,1)} %og_ref.1, bf16[128,256]{1,0:T(8,128)(2,1)} %x_ref.1, f32[2,128]{1,0:T(2,128)} %bitcast.19, ...), custom_call_target="tpu_custom_call" | custom-call | tf_op jit(solution)/shard_map/step/pallas_call | solution.py:582
  86.7 8.7 %grads.1 = (bf16[352,2048]{1,0:T(8,128)(2,1)}, bf16[352,2048]{1,0:T(8,128)(2,1)}, bf16[352,2048]{1,0:T(8,128)(2,1)}, f32[64,256]{1,0:T(8,128)}, bf16[128,256]{1,...) custom-call(bf16[2,512,2048]{2,1,0:T(8,128)(2,1)} %get-tuple-element.20.rows_ref, ...), custom_call_target="tpu_custom_call" | custom-call | tf_op jit(solution)/shard_map/grads/pallas_call | solution.py:673

commit v3 on v2

--- a/solution.py
+++ b/solution.py
@@ -15,12 +15,8 @@
 
 
 def block_order(nz):
-    order = [0]
-    for d in range(1, nz // 2 + 1):
-        order.append(d)
-        if nz - d != d:
-            order.append(nz - d)
-    return order[:nz]
+    near = [0, 1, nz - 1]
+    return near + sorted(set(range(nz)) - set(near), key=lambda d: (-min(d, nz - d), d))
 
 
 class Place:
@@ -37,6 +33,10 @@
         z = lax.rem(self.z + dz, self.nz)
         x = lax.rem(self.x + dx, NX)
         return (z * NX + x, self.tp)
+
+    def paired(self, dm, dx):
+        z = self.z + dm * (1 - 2 * lax.rem(self.z, 2))
+        return (z * NX + lax.rem(self.x + dx, NX), self.tp)
 
     def over_y(self, dy):
         return (self.sp, lax.rem(self.y + dy + NY, NY) * 2 + self.c)
@@ -157,8 +157,9 @@
     gradb_ref,
     gradc_ref,
     gradv_ref,
-    rows_hbm,
-    dt_hbm,
+    gate_ref,
+    up_ref,
+    down_ref,
     sbuf,
     buf,
     wcat,
@@ -252,12 +253,6 @@
         term = jnp.dot(places[k].astype(BF), weighted, preferred_element_type=F32)
         dy = term if dy is None else dy + term
     sbuf[1] = dy.astype(BF)
-    scol = lax.broadcasted_iota(jnp.int32, (tokens, total), 1).astype(F32)
-    pick[...] = ((scol == slots[0]).astype(F32) + (scol == slots[1]).astype(F32)).astype(BF)
-    mixed[...] = (gb_ref[...].astype(F32) * conv_ref[...].astype(F32)).astype(BF)
-    wcat[hid:padded, :] = jnp.zeros((padded - hid, wcat.shape[1]), BF)
-    wcat[padded + hid :, :] = jnp.zeros((padded - hid, wcat.shape[1]), BF)
-    wd[hid:, :] = jnp.zeros((padded - hid, wcat.shape[1]), BF)
 
     def cols(origin):
         return pl.ds(pl.multiple_of(origin * chans, chans), chans)
@@ -279,8 +274,17 @@
                     a_recv.at[p],
                     here.over_sp(dz, dx),
                 )
-    mrow = pl.ds(pl.multiple_of(here.x * tokens, tokens), tokens)
-    own_mixed = pltpu.make_async_copy(mixed, mx.at[mrow, :], own_sem.at[0])
+    scol = lax.broadcasted_iota(jnp.int32, (tokens, total), 1).astype(F32)
+    pick[...] = ((scol == slots[0]).astype(F32) + (scol == slots[1]).astype(F32)).astype(BF)
+    mixed[...] = (gb_ref[...].astype(F32) * conv_ref[...].astype(F32)).astype(BF)
+    wcat[hid:padded, :] = jnp.zeros((padded - hid, wcat.shape[1]), BF)
+    wcat[padded + hid :, :] = jnp.zeros((padded - hid, wcat.shape[1]), BF)
+    wd[hid:, :] = jnp.zeros((padded - hid, wcat.shape[1]), BF)
+
+    side = lax.rem(here.z, 2)
+    family = [(dm, dx) for dm in range(2) for dx in range(NX) if dm or dx]
+    seat = pl.ds(pl.multiple_of((side * NX + here.x) * tokens, tokens), tokens)
+    own_mixed = pltpu.make_async_copy(mixed, mx.at[seat, :], own_sem.at[0])
     own_mixed.start()
 
     def chunk(origin, h):
@@ -301,42 +305,6 @@
 
     def whole(k):
         return lambda origin: buf.at[:, pl.ds(k * half, half), cols(origin)]
-
-    def early(step):
-        if step == 0:
-            gather.finish(whole(0), 0)
-            for load in loads[:3]:
-                load.wait()
-        n = half // EARLY
-        if step < EARLY:
-            experts(step * n, n)
-
-    done = 0
-    for p in range(nz + LAST):
-        if p < nz:
-            if p == 0:
-                own.wait()
-                await_bytes(buf.at[:, cap:rows, column], a_recv.at[0])
-            else:
-                await_bytes(buf.at[:, pl.ds(p * rows, rows), column], a_recv.at[p])
-            gather.start(p)
-        if p == nz - 1:
-            for dx in range(1, NX):
-                send(mixed, mx.at[mrow, :], m_send, m_recv, here.over_sp(0, dx))
-        if 0 <= p - FORWARD < nz:
-            gather.forward(p - FORWARD)
-        if 0 <= p - LAST < nz:
-            gather.last(p - LAST)
-        if p >= hb + LAST and done < EARLY:
-            early(done)
-            done += 1
-    while done < EARLY:
-        early(done)
-        done += 1
-    gather.finish(whole(1), 1)
-    keep_rows = pltpu.make_async_copy(buf, rows_hbm, own_sem.at[6])
-    keep_rows.start()
-    experts(half, half)
 
     def spread(k):
         r = pl.ds(k * half, half)
@@ -354,9 +322,6 @@
                 here.other(),
             )
 
-    spread(1)
-    spread(0)
-
     def pair(p, dy):
         y = lax.rem(here.y + dy + NY, NY)
         r = pl.ds(p * rows, rows)
@@ -365,10 +330,6 @@
     def stage_a(p):
         way = 1 if p % 2 == 0 else -1
         r = pl.ds(p * rows, rows)
-        if p == nz - 1:
-            await_bytes(pr.at[:, pl.ds(half, half), :], pair_recv.at[1])
-        if p == hb - 1:
-            await_bytes(pr.at[:, pl.ds(0, half), :], pair_recv.at[0])
         sb[0, r, :] = pair(p, 2).astype(BF)
         send(sb.at[0, r, :], ra.at[r, :], rs_send.at[0], rs_recv.at[0, p], here.over_y(way))
         sb[1, r, :] = pair(p, -way).astype(BF)
@@ -394,22 +355,67 @@
             if dz or dx:
                 send(src, dst, sp_send, sp_recv, here.over_sp(dz, dx))
 
-    for s in range(nz + STAGE_C):
-        if s < nz:
-            stage_a(nz - 1 - s)
-        if 0 <= s - STAGE_B < nz:
-            stage_b(nz - 1 - (s - STAGE_B))
-        if 0 <= s - STAGE_C < nz:
-            stage_c(nz - 1 - (s - STAGE_C))
-    ret[0:cap, :] = fin[0:cap, :]
-
+    def pair_arrived(k):
+        await_bytes(pr.at[:, pl.ds(k * half, half), :], pair_recv.at[k])
+
+    first = list(range(hb - 1, -1, -1))
+    second = list(range(hb, nz))
+    for p in range(nz + LAST):
+        if p < nz:
+            if p == 0:
+                own.wait()
+                await_bytes(buf.at[:, cap:rows, column], a_recv.at[0])
+            else:
+                await_bytes(buf.at[:, pl.ds(p * rows, rows), column], a_recv.at[p])
+            gather.start(p)
+        if p == nz - 1:
+            for dm, dx in family:
+                send(mixed, mx.at[seat, :], m_send, m_recv, here.paired(dm, dx))
+        if 0 <= p - FORWARD < nz:
+            gather.forward(p - FORWARD)
+        if p == nz - 1 + FORWARD:
+            gather.finish(whole(0), 0)
+            for load in loads[:3]:
+                load.wait()
+            experts(0, half)
+        if 0 <= p - LAST < nz:
+            gather.last(p - LAST)
+        if p == nz + FORWARD:
+            spread(0)
+    pair_arrived(0)
+    for p in first:
+        stage_a(p)
+    gather.finish(whole(1), 1)
+    experts(half, half)
+    spread(1)
+    for p in first:
+        stage_b(p)
+    pair_arrived(1)
+    for p in second:
+        stage_a(p)
     slab = 3 * padded // 9
 
     def turn(k):
         dt[k * slab : (k + 1) * slab, :] = dcat[:, k * slab : (k + 1) * slab].astype(F32).T.astype(BF)
 
-    for k in range(3):
+    def weights(n):
+        c = pl.ds(n * chans, chans)
+        both = jnp.dot(dt[0 : 2 * padded, :], buf[0, :, c], preferred_element_type=F32)
+        gate_ref[:, c] = both[0:hid, :].astype(BF)
+        up_ref[:, c] = both[padded : padded + hid, :].astype(BF)
+        down_ref[:, c] = jnp.dot(dt[2 * padded :, :], buf[1, :, c], preferred_element_type=F32)[0:hid, :].astype(BF)
+
+    for p in first:
+        stage_c(p)
+    for k in range(9):
         turn(k)
+    for p in second:
+        stage_b(p)
+    for p in second:
+        stage_c(p)
+    ret[0:cap, :] = fin[0:cap, :]
+    for n in range(3):
+        weights(n)
     await_bytes(ret.at[pl.ds(cap, total - cap), :], sp_recv)
 
     moe = jnp.dot(pick[...], ret[...], preferred_element_type=F32)
@@ -418,22 +424,27 @@
     dh[...] = grad_h.astype(BF)
 
     wide = chans // NX
-    tcol = pl.ds(pl.multiple_of(here.x * tokens, tokens), tokens)
+    piece = wide // 2
+    tcol = pl.ds(pl.multiple_of((side * NX + here.x) * tokens, tokens), tokens)
 
     def orows(origin, h=0, n=1):
-        size = wide // n
-        return pl.ds(pl.multiple_of(origin * wide + h * size, size), size)
-
-    for dx in range(1, NX):
-        to = lax.rem(here.x + dx, NX)
+        size = piece // n
+        return pl.ds(pl.multiple_of(origin * piece + h * size, size), size)
+
+    def share(m, x):
+        return pl.ds(pl.multiple_of(x * wide + m * piece, piece), piece)
+
+    mine = orows(here.tp)
+    for dm, dx in family:
+        m = lax.rem(side + dm, 2)
         send(
-            dht.at[orows(to), :],
-            xall.at[orows(here.tp), tcol],
+            dht.at[share(m, lax.rem(here.x + dx, NX)), :],
+            xall.at[mine, tcol],
             x_send,
             x_recv,
-            here.over_sp(0, dx),
+            here.paired(dm, dx),
         )
-    own_x = pltpu.make_async_copy(dht.at[orows(here.x), :], xall.at[orows(here.tp), tcol], own_sem.at[1])
+    own_x = pltpu.make_async_copy(dht.at[share(side, here.x), :], xall.at[mine, tcol], own_sem.at[1])
     own_x.start()
     own_dh = pltpu.make_async_copy(dh, dhall.at[:, column], own_sem.at[2])
     own_dh.start()
@@ -443,22 +454,31 @@
     xb_gather = Gather(here, lambda o, h: xall.at[orows(o, h, 2), :], xb_send, xb_near, xb_far)
     dh_gather.start(0)
     dh_gather.start(1)
-    for k in range(3, 6):
-        turn(k)
+    weights(3)
     own_x.wait()
-    await_bytes(xall.at[pl.ds(0, wide), pl.ds(0, (NX - 1) * tokens)], x_recv)
+    await_bytes(xall.at[pl.ds(0, piece), pl.ds(0, len(family) * tokens)], x_recv)
     xb_gather.start(0)
     xb_gather.start(1)
+    weights(4)
+    weights(5)
     for h in range(2):
         dh_gather.forward(h)
     for h in range(2):
+        xb_gather.forward(h)
+    for h in range(2):
         dh_gather.last(h)
-    for k in range(6, 9):
-        turn(k)
-    keep_dt = pltpu.make_async_copy(dt, dt_hbm, own_sem.at[3])
-    keep_dt.start()
     for h in range(2):
-        xb_gather.forward(h)
+        xb_gather.last(h)
+    own_mixed.wait()
+    await_bytes(mx.at[pl.ds(0, len(family) * tokens), :], m_recv)
+    xb_gather.finish(lambda o: xall.at[orows(o), :])
+    gpart[...] = jnp.dot(xall[...], mx[...], preferred_element_type=F32).astype(BF)
+    for dz in order[1:]:
+        to = lax.rem(here.z + dz, nz)
+        send(gpart.at[orows(to), :], gr.at[dz], z_send, z_recv, here.over_sp(dz, 0))
+    own_g = pltpu.make_async_copy(gpart.at[orows(here.z), :], gr.at[0], own_sem.at[4])
+    own_g.start()
+
     dh_gather.finish(lambda o: dhall.at[:, cols(o)])
     loads[3].wait()
     grad_z = jnp.dot(dhall[...], out_proj[...], preferred_element_type=F32)
@@ -468,21 +488,11 @@
     last_sp = nz * NX
     before = (lax.rem(here.sp + last_sp - 1, last_sp), here.tp)
     after = (lax.rem(here.sp + 1, last_sp), here.tp)
-    for h in range(2):
-        xb_gather.last(h)
     send(edge.at[0], halo.at[1], e_send.at[0], e_recv.at[1], before)
     send(edge.at[1], halo.at[0], e_send.at[1], e_recv.at[0], after)
-    own_mixed.wait()
-    await_bytes(mx.at[pl.ds(0, (NX - 1) * tokens), :], m_recv)
-    xb_gather.finish(lambda o: xall.at[orows(o), :])
-    gpart[...] = jnp.dot(xall[...], mx[...], preferred_element_type=F32).astype(BF)
-    for dz in range(1, nz):
-        to = lax.rem(here.z + dz, nz)
-        send(gpart.at[orows(to), :], gr.at[dz], z_send, z_recv, here.over_sp(dz, 0))
-    own_g = pltpu.make_async_copy(gpart.at[orows(here.z), :], gr.at[0], own_sem.at[4])
-    own_g.start()
-
     gradb_ref[...] = (grad_z * conv_ref[...].astype(F32)).astype(BF)
+    for n in range(6, 2 * NY):
+        weights(n)
     await_bytes(halo.at[0], e_recv.at[0])
     await_bytes(halo.at[1], e_recv.at[1])
     dconv = dconv.astype(F32)
@@ -503,44 +513,35 @@
         await_bytes(ra, rs_send.at[k])
     await_bytes(ret.at[pl.ds(cap, total - cap), :], sp_send)
     await_bytes(dhall.at[:, pl.ds(0, others * chans)], dh_send)
-    await_bytes(xall.at[pl.ds(0, others * wide), :], xb_send)
-    await_bytes(xall.at[pl.ds(0, wide), pl.ds(0, (NX - 1) * tokens)], x_send)
-    await_bytes(mx.at[pl.ds(0, (NX - 1) * tokens), :], m_send)
+    await_bytes(xall.at[pl.ds(0, others * piece), :], xb_send)
+    await_bytes(xall.at[pl.ds(0, piece), pl.ds(0, len(family) * tokens)], x_send)
+    await_bytes(mx.at[pl.ds(0, len(family) * tokens), :], m_send)
     await_bytes(edge.at[0], e_send.at[0])
     await_bytes(edge.at[1], e_send.at[1])
-    keep_rows.wait()
-    keep_dt.wait()
 
     own_g.wait()
     await_bytes(gr.at[pl.ds(1, nz - 1)], z_recv)
-    summed = gr[0].astype(F32)
-    for k in range(1, nz):
-        summed = summed + gr[k].astype(F32)
-    go_ref[...] = summed
+    for m in range(2):
+        summed = gr[m].astype(F32)
+        for k in range(m + 2, nz, 2):
+            summed = summed + gr[k].astype(F32)
+        go_ref[pl.ds(pl.multiple_of(lax.rem(side + m, 2) * piece, piece), piece), :] = summed
     await_bytes(gr.at[pl.ds(1, nz - 1)], z_send)
 
 
-def grads_kernel(rows_ref, dt_ref, go, gb, gc, gv, gate_ref, up_ref, down_ref, go_ref, gb_ref, gc_ref, gv_ref):
-    hid, padded = gate_ref.shape[0], dt_ref.shape[0] // 3
-    x, dy = rows_ref[0], rows_ref[1]
-    both = jnp.dot(dt_ref[0 : 2 * padded, :], x, preferred_element_type=F32)
-    gate_ref[...] = both[0:hid, :].astype(BF)
-    up_ref[...] = both[padded : padded + hid, :].astype(BF)
-    down_ref[...] = jnp.dot(dt_ref[2 * padded :, :], dy, preferred_element_type=F32)[0:hid, :].astype(BF)
-
-    @pl.when(pl.program_id(0) == 0)
-    def _():
-        go_ref[...] = go[...]
-        gb_ref[...] = gb[...]
-        gc_ref[...] = gc[...]
-        gv_ref[...] = gv[...]
+def write_kernel(*refs):
+    count = len(refs) // 2
+    sems = refs[-1]
+    copies = [pltpu.make_async_copy(refs[k], refs[count + k], sems.at[k]) for k in range(count)]
+    for copy in copies:
+        copy.start()
+    for copy in copies:
+        copy.wait()
 
 
 VM = pl.BlockSpec(memory_space=pltpu.VMEM)
 ANY = pl.BlockSpec(memory_space=pl.ANY)
 FORWARD, LAST = 2, 4
-STAGE_B, STAGE_C = 2, 4
-EARLY = 2
 
 
 def local(
@@ -579,15 +580,13 @@
         jax.ShapeDtypeStruct((tokens, chans), BF),
         jax.ShapeDtypeStruct((tokens, chans), BF),
     ]
-    *results, kept_rows, kept_dt = pl.pallas_call(
+    held = [(a.shape, a.dtype) for a in small]
+    held += [((hid, width), BF)] * 3
+    results = pl.pallas_call(
         functools.partial(step_kernel, nz),
-        out_shape=[
-            *small,
-            jax.ShapeDtypeStruct((2, total, width), BF),
-            jax.ShapeDtypeStruct((3 * padded, total), BF),
-        ],
+        out_shape=[pltpu.VMEM(*h) for h in held],
         in_specs=[VM] * 9 + [ANY] * 4,
-        out_specs=[VM] * 4 + [ANY] * 2,
+        out_specs=[VM] * 7,
         scratch_shapes=[
             vm(2, total, chans),
             vm(2, total, width),
@@ -609,13 +608,13 @@
             vm(tokens, chans),
             vm(tokens, width),
             vm(chans, tokens),
-            vm(ntp * wide, NX * tokens),
+            vm(ntp * wide // 2, 2 * NX * tokens),
             vm(tokens, chans),
-            vm(NX * tokens, chans),
+            vm(2 * NX * tokens, chans),
             vm(2, 16, chans),
             vm(2, 16, chans),
-            vm(nz * wide, chans),
-            vm(nz, wide, chans),
+            vm(nz * wide // 2, chans),
+            vm(nz, wide // 2, chans),
             dma((4,)),
             dma((7,)),
             dma,
@@ -645,40 +644,38 @@
             dma,
         ],
         compiler_params=pltpu.CompilerParams(
-            collective_id=0, has_side_effects=True, vmem_limit_bytes=60 * 1024 * 1024
+            collective_id=0, has_side_effects=True, vmem_limit_bytes=40 * 1024 * 1024
         ),
         name="step",
     )(
-        out_grad,
-        moe_input,
-        route_weight.T,
-        route_ids.T,
-        conv_out,
-        gate_b,
-        gate_c,
-        value_v,
-        conv_taps,
-        gate_proj[0].T,
-        up_proj[0].T,
-        down_proj[0],
-        out_proj,
+        *(
+            pltpu.with_memory_space_constraint(a, pltpu.HBM)
+            for a in (
+                out_grad,
+                moe_input,
+                route_weight.T,
+                route_ids.T,
+                conv_out,
+                gate_b,
+                gate_c,
+                value_v,
+                conv_taps,
+                gate_proj[0].T,
+                up_proj[0].T,
+                down_proj[0],
+                out_proj,
+            )
+        )
     )
-
-    step = width // 8
-
-    def held(shape):
-        return pl.BlockSpec(shape, lambda i: (0, 0))
-
-    weights = pl.BlockSpec((hid, step), lambda i: (0, i))
-    grad_gate, grad_up, grad_down, grad_out, grad_b, grad_c, grad_v = pl.pallas_call(
-        grads_kernel,
-        grid=(width // step,),
-        out_shape=[jax.ShapeDtypeStruct((hid, width), BF)] * 3 + small,
-        in_specs=[pl.BlockSpec((2, total, step), lambda i: (0, 0, i)), held(kept_dt.shape)]
-        + [held(s.shape) for s in small],
-        out_specs=[weights] * 3 + [held(s.shape) for s in small],
-        name="grads",
-    )(kept_rows, kept_dt, *results)
+    grad_out, grad_b, grad_c, grad_v, grad_gate, grad_up, grad_down = pl.pallas_call(
+        write_kernel,
+        out_shape=[jax.ShapeDtypeStruct(*h) for h in held],
+        in_specs=[VM] * 7,
+        out_specs=[ANY] * 7,
+        scratch_shapes=[dma((7,))],
+        compiler_params=pltpu.CompilerParams(vmem_limit_bytes=8 * 1024 * 1024),
+        name="write",
+    )(*[pltpu.with_memory_space_constraint(r, pltpu.VMEM) for r in results])
     return (grad_gate.T[None], grad_up.T[None], grad_down[None], grad_out, grad_b, grad_c, grad_v)
 
 

time: 95.8 us -> 80.5 us (0.84)
  Pallas kernels: 94.8 us -> 79.7 us
    pallas_call x2, Pallas kernels: 94.8 us -> 79.7 us  [the longest x1 77.5 us: local(): pl.pallas_call(functools.partial(step_kernel, nz), out_shape=[pltpu.VMEM(...]
where the time goes in v3:
time: 80.5 us; the launch traced here: 80.4 us
  Pallas kernels  79.7 us (99%)
    pallas_call x1, Pallas kernels, local(): pl.pallas_call(functools.partial(step_kernel, nz), out_shape=[pltpu.VMEM(...  77.5 us
    pallas_call x1, Pallas kernels, local(): pl.pallas_call(write_kernel, out_shape=[jax.ShapeDtypeStruct(*h) for h in...  2.2 us

profile of v3, /device:TPU:1, one launch (start us, length us, event | category | flops | bytes accessed | tf_op | source)
XLA Modules:
  0.0 80.4 jit_solution(16853002486333884676)
XLA Ops:
  0.6 77.5 %step.1 = (f32[64,256]{1,0:T(8,128)S(1)}, bf16[128,256]{1,0:T(8,128)(2,1)S(1)}, bf16[128,256]{1,0:T(8,128)(2,1)S(1)}, bf16[128,256]{1,0:T(8,128)(2,1)S(1)}, bf16...) custom-call(bf16[128,256]{1,0:T(8,128)(2,1)} %og_ref.1, ...), custom_call_target="tpu_custom_call" | custom-call | tf_op jit(solution)/shard_map/step/pallas_call | solution.py:585
  78.2 2.2 %write.1 = (f32[64,256]{1,0:T(8,128)}, bf16[128,256]{1,0:T(8,128)(2,1)}, bf16[128,256]{1,0:T(8,128)(2,1)}, bf16[128,256]{1,0:T(8,128)(2,1)}, bf16[352,2048]{1,0:...) custom-call(f32[64,256]{1,0:T(8,128)S(1)} %get-tuple-element.21.refs_0_, ...), custom_call_target="tpu_custom_call" | custom-call | tf_op jit(solution)/shard_map/write/pallas_call | solution.py:670

commit v4 on v3

--- a/solution.py
+++ b/solution.py
@@ -53,7 +53,7 @@
 def greet(here):
     barrier = pltpu.get_barrier_semaphore()
     peers = [here.over_sp(dz, dx) for dz in range(here.nz) for dx in range(NX) if dz or dx]
-    peers += [here.other(), here.over_y(1), here.over_y(-1)]
+    peers += [here.other(), here.over_y(1), here.over_y(-1), here.over_y(2)]
     for peer in peers:
         pl.semaphore_signal(barrier, inc=1, device_id=peer, device_id_type=MESH)
     return barrier, len(peers)
@@ -76,9 +76,9 @@
 
 
 class Gather:
-    def __init__(self, here, chunk, send_sem, near, far, group=lambda h: 0):
+    def __init__(self, here, chunk, send_sem, near, far, group=lambda h: 0, direct=False):
         self.here, self.chunk, self.send_sem = here, chunk, send_sem
-        self.near, self.far, self.group = near, far, group
+        self.near, self.far, self.group, self.direct = near, far, group, direct
 
     def _send(self, origin, h, peer, recv_sem):
         ref = self.chunk(origin, h)
@@ -89,17 +89,19 @@
         mine = here.origin(0, False)
         self._send(mine, h, here.over_y(1), self.near.at[0, h])
         self._send(mine, h, here.over_y(-1), self.near.at[1, h])
+        if self.direct:
+            self._send(mine, h, here.over_y(2), self.near.at[2, h])
         self._send(mine, h, here.other(), self.far.at[0, self.group(h)])
 
     def forward(self, h):
         here = self.here
         low, high = here.origin(-1, False), here.origin(1, False)
         await_bytes(self.chunk(low, h), self.near.at[0, h])
-        if h % 2 == 0:
+        if h % 2 == 0 and not self.direct:
             self._send(low, h, here.over_y(1), self.near.at[2, h])
         self._send(low, h, here.other(), self.far.at[1, self.group(h)])
         await_bytes(self.chunk(high, h), self.near.at[1, h])
-        if h % 2 == 1:
+        if h % 2 == 1 and not self.direct:
             self._send(high, h, here.over_y(-1), self.near.at[2, h])
         self._send(high, h, here.other(), self.far.at[2, self.group(h)])
 
@@ -140,15 +142,15 @@
 
 def step_kernel(
     nz,
-    og_ref,
-    x_ref,
-    rw_ref,
-    ids_ref,
-    conv_ref,
-    gb_ref,
-    gc_ref,
-    vv_ref,
-    taps_ref,
+    og_hbm,
+    x_hbm,
+    rw_hbm,
+    ids_hbm,
+    conv_hbm,
+    gb_hbm,
+    gc_hbm,
+    vv_hbm,
+    taps_hbm,
     wg_hbm,
     wu_hbm,
     wd_hbm,
@@ -160,6 +162,15 @@
     gate_ref,
     up_ref,
     down_ref,
+    og_ref,
+    x_ref,
+    rw_ref,
+    ids_ref,
+    conv_ref,
+    gb_ref,
+    gc_ref,
+    vv_ref,
+    taps_ref,
     sbuf,
     buf,
     wcat,
@@ -187,6 +198,7 @@
     halo,
     gpart,
     gr,
+    i_sem,
     w_sem,
     own_sem,
     a_send,
@@ -227,6 +239,24 @@
     half = total // 2
     hb = nz // 2
 
+    inputs = [
+        pltpu.make_async_copy(a, b, i_sem.at[k])
+        for k, (a, b) in enumerate(
+            [
+                (ids_hbm, ids_ref),
+                (rw_hbm, rw_ref),
+                (x_hbm, x_ref),
+                (og_hbm, og_ref),
+                (gb_hbm, gb_ref),
+                (conv_hbm, conv_ref),
+                (gc_hbm, gc_ref),
+                (vv_hbm, vv_ref),
+                (taps_hbm, taps_ref),
+            ]
+        )
+    ]
+    for load in inputs:
+        load.start()
     loads = [
         pltpu.make_async_copy(wg_hbm, wcat.at[0:hid, :], w_sem.at[0]),
         pltpu.make_async_copy(wu_hbm, wcat.at[padded : padded + hid, :], w_sem.at[1]),
@@ -236,8 +266,8 @@
     for load in loads:
         load.start()
 
+    inputs[0].wait()
     ids = ids_ref[...].astype(F32).T.astype(jnp.int32)
-    rw = rw_ref[...].T
     slots = slots_of(ids, here, total)
     srow = lax.broadcasted_iota(jnp.int32, (total, tokens), 0).astype(F32)
     places = []
@@ -245,6 +275,9 @@
         wide = jnp.broadcast_to(slots[k], (tokens, tokens)).T
         places.append((srow == wide[0:1, :]).astype(F32))
     both = (places[0] + places[1]).astype(BF)
+    for load in inputs[1:4]:
+        load.wait()
+    rw = rw_ref[...].T
     sbuf[0] = jnp.dot(both, x_ref[...], preferred_element_type=F32).astype(BF)
     og = og_ref[...].astype(F32)
     dy = None
@@ -276,6 +309,8 @@
                 )
     scol = lax.broadcasted_iota(jnp.int32, (tokens, total), 1).astype(F32)
     pick[...] = ((scol == slots[0]).astype(F32) + (scol == slots[1]).astype(F32)).astype(BF)
+    for load in inputs[4:]:
+        load.wait()
     mixed[...] = (gb_ref[...].astype(F32) * conv_ref[...].astype(F32)).astype(BF)
     wcat[hid:padded, :] = jnp.zeros((padded - hid, wcat.shape[1]), BF)
     wcat[padded + hid :, :] = jnp.zeros((padded - hid, wcat.shape[1]), BF)
@@ -309,18 +344,13 @@
     def spread(k):
         r = pl.ds(k * half, half)
         d = dcat[r, 0 : 2 * padded]
-        step = 2 * chans
-        for n in range(NY):
-            c = pl.ds(n * step, step)
-            part[r, c] = jnp.dot(d, wcat[:, c], preferred_element_type=F32).astype(BF)
-        for y in range(NY):
-            send(
-                part.at[r, cols(2 * y + 1 - here.c)],
-                pr.at[y, r, :],
-                pair_send,
-                pair_recv.at[k],
-                here.other(),
-            )
+        for first_y in range(0, NY, 2):
+            for y in range(first_y, first_y + 2):
+                c = pl.ds(2 * y * chans, 2 * chans)
+                part[r, c] = jnp.dot(d, wcat[:, c], preferred_element_type=F32).astype(BF)
+            for y in range(first_y, first_y + 2):
+                at = cols(2 * y + 1 - here.c)
+                send(part.at[r, at], pr.at[y, r, :], pair_send, pair_recv.at[k], here.other())
 
     def pair(p, dy):
         y = lax.rem(here.y + dy + NY, NY)
@@ -373,14 +403,14 @@
                 send(mixed, mx.at[seat, :], m_send, m_recv, here.paired(dm, dx))
         if 0 <= p - FORWARD < nz:
             gather.forward(p - FORWARD)
-        if p == nz - 1 + FORWARD:
+        if p == EXPERTS_AT:
             gather.finish(whole(0), 0)
             for load in loads[:3]:
                 load.wait()
             experts(0, half)
         if 0 <= p - LAST < nz:
             gather.last(p - LAST)
-        if p == nz + FORWARD:
+        if p == SPREAD_AT:
             spread(0)
     pair_arrived(0)
     for p in first:
@@ -451,7 +481,7 @@
     own_dh.wait()
     ht = tokens // 2
     dh_gather = Gather(here, lambda o, h: dhall.at[pl.ds(h * ht, ht), cols(o)], dh_send, dh_near, dh_far)
-    xb_gather = Gather(here, lambda o, h: xall.at[orows(o, h, 2), :], xb_send, xb_near, xb_far)
+    xb_gather = Gather(here, lambda o, h: xall.at[orows(o, h, 2), :], xb_send, xb_near, xb_far, direct=DIRECT)
     dh_gather.start(0)
     dh_gather.start(1)
     weights(3)
@@ -469,16 +499,6 @@
         dh_gather.last(h)
     for h in range(2):
         xb_gather.last(h)
-    own_mixed.wait()
-    await_bytes(mx.at[pl.ds(0, len(family) * tokens), :], m_recv)
-    xb_gather.finish(lambda o: xall.at[orows(o), :])
-    gpart[...] = jnp.dot(xall[...], mx[...], preferred_element_type=F32).astype(BF)
-    for dz in order[1:]:
-        to = lax.rem(here.z + dz, nz)
-        send(gpart.at[orows(to), :], gr.at[dz], z_send, z_recv, here.over_sp(dz, 0))
-    own_g = pltpu.make_async_copy(gpart.at[orows(here.z), :], gr.at[0], own_sem.at[4])
-    own_g.start()
-
     dh_gather.finish(lambda o: dhall.at[:, cols(o)])
     loads[3].wait()
     grad_z = jnp.dot(dhall[...], out_proj[...], preferred_element_type=F32)
@@ -491,6 +511,16 @@
     send(edge.at[0], halo.at[1], e_send.at[0], e_recv.at[1], before)
     send(edge.at[1], halo.at[0], e_send.at[1], e_recv.at[0], after)
     gradb_ref[...] = (grad_z * conv_ref[...].astype(F32)).astype(BF)
+    own_mixed.wait()
+    await_bytes(mx.at[pl.ds(0, len(family) * tokens), :], m_recv)
+    xb_gather.finish(lambda o: xall.at[orows(o), :])
+    gpart[...] = jnp.dot(xall[...], mx[...], preferred_element_type=F32).astype(BF)
+    for dz in sorted(range(1, nz), key=lambda d: -min(d, nz - d)):
+        to = lax.rem(here.z + dz, nz)
+        send(gpart.at[orows(to), :], gr.at[dz], z_send, z_recv, here.over_sp(dz, 0))
+    own_g = pltpu.make_async_copy(gpart.at[orows(here.z), :], gr.at[0], own_sem.at[4])
+    own_g.start()
+
     for n in range(6, 2 * NY):
         weights(n)
     await_bytes(halo.at[0], e_recv.at[0])
@@ -541,7 +571,9 @@
 
 VM = pl.BlockSpec(memory_space=pltpu.VMEM)
 ANY = pl.BlockSpec(memory_space=pl.ANY)
+DIRECT = True
 FORWARD, LAST = 2, 4
+EXPERTS_AT, SPREAD_AT = 8, 9
 
 
 def local(
@@ -585,9 +617,18 @@
     results = pl.pallas_call(
         functools.partial(step_kernel, nz),
         out_shape=[pltpu.VMEM(*h) for h in held],
-        in_specs=[VM] * 9 + [ANY] * 4,
+        in_specs=[ANY] * 13,
         out_specs=[VM] * 7,
         scratch_shapes=[
+            vm(tokens, chans),
+            vm(tokens, chans),
+            pltpu.VMEM((2, tokens), F32),
+            pltpu.VMEM((2, tokens), jnp.int32),
+            vm(tokens, chans),
+            vm(tokens, chans),
+            vm(tokens, chans),
+            vm(tokens, chans),
+            pltpu.VMEM(conv_taps.shape, F32),
             vm(2, total, chans),
             vm(2, total, width),
             vm(2 * padded, width),
@@ -615,6 +656,7 @@
             vm(2, 16, chans),
             vm(nz * wide // 2, chans),
             vm(nz, wide // 2, chans),
+            dma((9,)),
             dma((4,)),
             dma((7,)),
             dma,

time: 80.5 us -> 78.9 us (0.980)
  Pallas kernels: 79.7 us -> 78.2 us
    pallas_call x1, Pallas kernels: 77.5 us -> 76 us  [local(): pl.pallas_call(functools.partial(step_kernel, nz), out_shape=[pltpu.VMEM(...]
where the time goes in v4:
time: 78.9 us
  Pallas kernels  78.2 us (99%)
    pallas_call x1, Pallas kernels, local(): pl.pallas_call(functools.partial(step_kernel, nz), out_shape=[pltpu.VMEM(...  76 us
    pallas_call x1, Pallas kernels, local(): pl.pallas_call(write_kernel, out_shape=[jax.ShapeDtypeStruct(*h) for h in...  2.2 us

profile of v4, /device:TPU:1, one launch (start us, length us, event | category | flops | bytes accessed | tf_op | source)
XLA Modules:
  0.0 78.9 jit_solution(10513712617162855754)
XLA Ops:
  0.6 76.0 %step.1 = (f32[64,256]{1,0:T(8,128)S(1)}, bf16[128,256]{1,0:T(8,128)(2,1)S(1)}, bf16[128,256]{1,0:T(8,128)(2,1)S(1)}, bf16[128,256]{1,0:T(8,128)(2,1)S(1)}, bf16...) custom-call(bf16[128,256]{1,0:T(8,128)(2,1)} %og_hbm.1, ...), custom_call_target="tpu_custom_call" | custom-call | tf_op jit(solution)/shard_map/step/pallas_call | solution.py:617
  76.7 2.2 %write.1 = (f32[64,256]{1,0:T(8,128)}, bf16[128,256]{1,0:T(8,128)(2,1)}, bf16[128,256]{1,0:T(8,128)(2,1)}, bf16[128,256]{1,0:T(8,128)(2,1)}, bf16[352,2048]{1,0:...) custom-call(f32[64,256]{1,0:T(8,128)S(1)} %get-tuple-element.21.refs_0_, ...), custom_call_target="tpu_custom_call" | custom-call | tf_op jit(solution)/shard_map/write/pallas_call | solution.py:712

commit v5 on v4

--- a/solution.py
+++ b/solution.py
@@ -76,9 +76,9 @@
 
 
 class Gather:
-    def __init__(self, here, chunk, send_sem, near, far, group=lambda h: 0, direct=False):
+    def __init__(self, here, chunk, send_sem, near, far, group=lambda h: 0, part=None):
         self.here, self.chunk, self.send_sem = here, chunk, send_sem
-        self.near, self.far, self.group, self.direct = near, far, group, direct
+        self.near, self.far, self.group, self.part = near, far, group, part
 
     def _send(self, origin, h, peer, recv_sem):
         ref = self.chunk(origin, h)
@@ -89,26 +89,35 @@
         mine = here.origin(0, False)
         self._send(mine, h, here.over_y(1), self.near.at[0, h])
         self._send(mine, h, here.over_y(-1), self.near.at[1, h])
-        if self.direct:
+        if self.part is None:
             self._send(mine, h, here.over_y(2), self.near.at[2, h])
         self._send(mine, h, here.other(), self.far.at[0, self.group(h)])
 
-    def forward(self, h):
+    def forward(self, h, between=None):
         here = self.here
         low, high = here.origin(-1, False), here.origin(1, False)
         await_bytes(self.chunk(low, h), self.near.at[0, h])
-        if h % 2 == 0 and not self.direct:
-            self._send(low, h, here.over_y(1), self.near.at[2, h])
+        self._pass(low, h, 0, here.over_y(1))
         self._send(low, h, here.other(), self.far.at[1, self.group(h)])
+        if between is not None:
+            between()
         await_bytes(self.chunk(high, h), self.near.at[1, h])
-        if h % 2 == 1 and not self.direct:
-            self._send(high, h, here.over_y(-1), self.near.at[2, h])
+        self._pass(high, h, 1, here.over_y(-1))
         self._send(high, h, here.other(), self.far.at[2, self.group(h)])
+
+    def _pass(self, origin, h, k, peer):
+        if self.part is not None:
+            ref = self.part(origin, h, k)
+            send(ref, ref, self.send_sem, self.near.at[2 + k, h], peer)
 
     def last(self, h):
         here = self.here
         across = here.origin(2, False)
-        await_bytes(self.chunk(across, h), self.near.at[2, h])
+        if self.part is None:
+            await_bytes(self.chunk(across, h), self.near.at[2, h])
+        else:
+            for k in range(2):
+                await_bytes(self.part(across, h, k), self.near.at[2 + k, h])
         self._send(across, h, here.other(), self.far.at[3, self.group(h)])
 
     def finish(self, whole, g=0):
@@ -176,6 +185,8 @@
     wcat,
     wd,
     out_proj,
+    gu,
+    dhid_s,
     dcat,
     dt,
     part,
@@ -294,7 +305,7 @@
     pl.semaphore_wait(barrier, peers)
     own = pltpu.make_async_copy(sbuf.at[:, 0:cap, :], buf.at[:, 0:cap, column], own_sem.at[5])
     own.start()
-    for dz in order:
+    for dz in [(-d) % nz for d in order]:
         for dx in range(NX):
             if dz or dx:
                 r = (dz * NX + dx) * cap
@@ -325,32 +336,42 @@
     def chunk(origin, h):
         return buf.at[:, pl.ds(h * rows, rows), cols(origin)]
 
-    gather = Gather(here, chunk, g_send, g_near, g_far, lambda h: h // hb)
-
-    def experts(r0, n):
-        r = pl.ds(r0, n)
-        gu = nt(buf[0, r, :], wcat[...])
-        dhid = nt(buf[1, r, :], wd[...])
-        gate, upval = gu[:, :padded], gu[:, padded:]
-        sig = jax.nn.sigmoid(gate)
-        act = gate * sig
-        dcat[r, 0:padded] = (dhid * upval * (sig * (1.0 + gate * (1.0 - sig)))).astype(BF)
-        dcat[r, padded : 2 * padded] = (dhid * act).astype(BF)
-        dcat[r, 2 * padded :] = (act * upval).astype(BF)
+    def part_of(origin, h, k):
+        return buf.at[k, pl.ds(h * rows, rows), cols(origin)]
+
+    gather = Gather(here, chunk, g_send, g_near, g_far, lambda h: h // hb, part_of)
+
+    def hidden_units(r0):
+        r = pl.ds(r0, half)
+
+        def ahead():
+            gu[...] = nt(buf[0, r, :], wcat[...])
+
+        def back():
+            dhid_s[...] = nt(buf[1, r, :], wd[...])
+
+        def combine():
+            gate, upval, dhid = gu[:, :padded], gu[:, padded:], dhid_s[...]
+            sig = jax.nn.sigmoid(gate)
+            act = gate * sig
+            dcat[r, 0:padded] = (dhid * upval * (sig * (1.0 + gate * (1.0 - sig)))).astype(BF)
+            dcat[r, padded : 2 * padded] = (dhid * act).astype(BF)
+            dcat[r, 2 * padded :] = (act * upval).astype(BF)
+
+        return ahead, back, combine
 
     def whole(k):
         return lambda origin: buf.at[:, pl.ds(k * half, half), cols(origin)]
 
-    def spread(k):
+    def spread(k, first_y):
         r = pl.ds(k * half, half)
         d = dcat[r, 0 : 2 * padded]
-        for first_y in range(0, NY, 2):
-            for y in range(first_y, first_y + 2):
-                c = pl.ds(2 * y * chans, 2 * chans)
-                part[r, c] = jnp.dot(d, wcat[:, c], preferred_element_type=F32).astype(BF)
-            for y in range(first_y, first_y + 2):
-                at = cols(2 * y + 1 - here.c)
-                send(part.at[r, at], pr.at[y, r, :], pair_send, pair_recv.at[k], here.other())
+        for y in range(first_y, first_y + 2):
+            c = pl.ds(2 * y * chans, 2 * chans)
+            part[r, c] = jnp.dot(d, wcat[:, c], preferred_element_type=F32).astype(BF)
+        for y in range(first_y, first_y + 2):
+            at = cols(2 * y + 1 - here.c)
+            send(part.at[r, at], pr.at[y, r, :], pair_send, pair_recv.at[k], here.other())
 
     def pair(p, dy):
         y = lax.rem(here.y + dy + NY, NY)
@@ -402,22 +423,27 @@
             for dm, dx in family:
                 send(mixed, mx.at[seat, :], m_send, m_recv, here.paired(dm, dx))
         if 0 <= p - FORWARD < nz:
-            gather.forward(p - FORWARD)
+            gather.forward(p - FORWARD, back if p == EXPERTS_AT + 1 else None)
         if p == EXPERTS_AT:
             gather.finish(whole(0), 0)
             for load in loads[:3]:
                 load.wait()
-            experts(0, half)
+            ahead, back, combine = hidden_units(0)
+            ahead()
+        if p == EXPERTS_AT + 1:
+            combine()
         if 0 <= p - LAST < nz:
             gather.last(p - LAST)
-        if p == SPREAD_AT:
-            spread(0)
+        if p > EXPERTS_AT and p < EXPERTS_AT + 3:
+            spread(0, 2 * (p - EXPERTS_AT - 1))
     pair_arrived(0)
     for p in first:
         stage_a(p)
     gather.finish(whole(1), 1)
-    experts(half, half)
-    spread(1)
+    for task in hidden_units(half):
+        task()
+    spread(1, 0)
+    spread(1, 2)
     for p in first:
         stage_b(p)
     pair_arrived(1)
@@ -481,7 +507,7 @@
     own_dh.wait()
     ht = tokens // 2
     dh_gather = Gather(here, lambda o, h: dhall.at[pl.ds(h * ht, ht), cols(o)], dh_send, dh_near, dh_far)
-    xb_gather = Gather(here, lambda o, h: xall.at[orows(o, h, 2), :], xb_send, xb_near, xb_far, direct=DIRECT)
+    xb_gather = Gather(here, lambda o, h: xall.at[orows(o, h, 2), :], xb_send, xb_near, xb_far)
     dh_gather.start(0)
     dh_gather.start(1)
     weights(3)
@@ -571,9 +597,8 @@
 
 VM = pl.BlockSpec(memory_space=pltpu.VMEM)
 ANY = pl.BlockSpec(memory_space=pl.ANY)
-DIRECT = True
 FORWARD, LAST = 2, 4
-EXPERTS_AT, SPREAD_AT = 8, 9
+EXPERTS_AT = 8
 
 
 def local(
@@ -634,6 +659,8 @@
             vm(2 * padded, width),
             vm(padded, width),
             vm(width, chans),
+            pltpu.VMEM((total // 2, 2 * padded), F32),
+            pltpu.VMEM((total // 2, padded), F32),
             vm(total, 3 * padded),
             vm(3 * padded, total),
             vm(total, width),
@@ -662,7 +689,7 @@
             dma,
             dma((nz,)),
             dma,
-            dma((3, nz)),
+            dma((4, nz)),
             dma((4, 2)),
             dma,
             dma((2,)),

time: 78.9 us -> 78 us (0.989)
  Pallas kernels: 78.2 us -> 77.3 us
    pallas_call x1, Pallas kernels: 76 us -> 75.1 us  [local(): pl.pallas_call(functools.partial(step_kernel, nz), out_shape=[pltpu.VMEM(...]
where the time goes in v5:
time: 78 us; the launch traced here: 77.9 us
  Pallas kernels  77.3 us (99%)
    pallas_call x1, Pallas kernels, local(): pl.pallas_call(functools.partial(step_kernel, nz), out_shape=[pltpu.VMEM(...  75.1 us
    pallas_call x1, Pallas kernels, local(): pl.pallas_call(write_kernel, out_shape=[jax.ShapeDtypeStruct(*h) for h in...  2.2 us

profile of v5, /device:TPU:1, one launch (start us, length us, event | category | flops | bytes accessed | tf_op | source)
XLA Modules:
  0.0 77.9 jit_solution(9323211959024066217)
XLA Ops:
  0.6 75.1 %step.1 = (f32[64,256]{1,0:T(8,128)S(1)}, bf16[128,256]{1,0:T(8,128)(2,1)S(1)}, bf16[128,256]{1,0:T(8,128)(2,1)S(1)}, bf16[128,256]{1,0:T(8,128)(2,1)S(1)}, bf16...) custom-call(bf16[128,256]{1,0:T(8,128)(2,1)} %og_hbm.1, ...), custom_call_target="tpu_custom_call" | custom-call | tf_op jit(solution)/shard_map/step/pallas_call | solution.py:642
  75.7 2.2 %write.1 = (f32[64,256]{1,0:T(8,128)}, bf16[128,256]{1,0:T(8,128)(2,1)}, bf16[128,256]{1,0:T(8,128)(2,1)}, bf16[128,256]{1,0:T(8,128)(2,1)}, bf16[352,2048]{1,0:...) custom-call(f32[64,256]{1,0:T(8,128)S(1)} %get-tuple-element.21.refs_0_, ...), custom_call_target="tpu_custom_call" | custom-call | tf_op jit(solution)/shard_map/write/pallas_call | solution.py:739
